TPU v7x, 32 devices: a whole 2x2x4 slice. The times are simulated.
32 devices in a mesh: ep: 8 (over z, x), tp: 4 (over y, core).
Axes of the slice: x: 2, y: 2, z: 4, core: 2. Of those that a mesh axis runs over, the one named last changes fastest.
Arguments:
- tokens: bfloat16 [1024, 2048], P('ep'), may hold values from -16 to 16
- routes: int32 [1024, 2], P('ep'), may hold values from 0 to 7, all different within a row; in each aligned block of 128 rows (0 to 127, 128 to 255, ...) at most 48 rows name the same one
- router: bfloat16 [2048, 8], replicated, may hold values from -0.125 to 0.125
- w_gate: bfloat16 [8, 2048, 2048], P('ep', None, 'tp'), may hold values from -0.125 to 0.125
- w_up: bfloat16 [8, 2048, 2048], P('ep', None, 'tp'), may hold values from -0.125 to 0.125
- w_down: bfloat16 [8, 2048, 2048], P('ep', 'tp'), may hold values from -0.125 to 0.125
- cotangent: bfloat16 [1024, 2048], P('ep'), may hold values from -6 to 6
Outputs:
- grad_tokens: bfloat16 [1024, 2048], P('ep', 'tp')
- grad_router: float32 [2048, 8], P('tp')
- grad_gate: float32 [8, 2048, 2048], P('ep', None, 'tp')
- grad_up: float32 [8, 2048, 2048], P('ep', None, 'tp')
- grad_down: float32 [8, 2048, 2048], P('ep', 'tp')
Inputs may be any that keep to these rules, and one draw needn't show every extreme that they name: In each aligned block of 128 rows, no expert is named by more than 48 of the block's routes, a bound that some block reaches; a row names 2 different experts.
All inputs are finite; a program needn't handle non-finite values.
Results may differ from a plain program's by a relative error of at most 0.017.
Values may be sent and summed in bfloat16 or wider, within the bound.
No kernel may reach another device: no remote copies, remote signals or barrier semaphores. Data moves between devices by JAX's collectives and lax.ppermute only.
A program may use at most 128 MiB of HBM per device.

v0:
```python
import functools
import math

import jax
import jax.numpy as jnp
from jax import lax
from jax.experimental import pallas as pl
from jax.experimental.pallas import tpu as pltpu
from jax.sharding import PartitionSpec as P


clamp_limit = 7.0
sig_slope = 1.702
cores = 2
groups = 2
lanes = 128
vmem_grant = 16 * 2**20


f32, bf16, i32 = jnp.float32, jnp.bfloat16, jnp.int32


def round_up(value, step):
    return -(-value // step) * step


def call(kernel, outs, args, flops, scratch=(), in_hbm=(), aliases=None, out_in_hbm=()):
    vmem, hbm = pl.BlockSpec(memory_space=pltpu.VMEM), pl.BlockSpec(memory_space=pltpu.HBM)
    args = [pltpu.with_memory_space_constraint(a, pltpu.HBM) if i in in_hbm else a for i, a in enumerate(args)]
    moved = sum(a.size * a.dtype.itemsize for a in args) + sum(2 * math.prod(o.shape) for o in outs)
    return pl.pallas_call(
        kernel,
        out_shape=outs,
        in_specs=[hbm if i in in_hbm else vmem for i in range(len(args))],
        out_specs=[hbm if i in out_in_hbm else vmem for i in range(len(outs))],
        scratch_shapes=list(scratch),
        input_output_aliases=aliases or {},
        compiler_params=pltpu.CompilerParams(vmem_limit_bytes=vmem_grant),
        cost_estimate=pl.CostEstimate(flops=flops, bytes_accessed=moved, transcendentals=0),
    )(*args)


def shaped(shape, dtype):
    return jax.ShapeDtypeStruct(shape, dtype)


def dot(a, b, contract):
    return lax.dot_general(a, b, ((contract[:1], contract[1:]), ((), ())), preferred_element_type=f32)


def iota(shape, axis):
    return lax.broadcasted_iota(i32, shape, axis)


def power_block(count):
    return count & -count


def moved_to(index, step, ep_count, sign):
    turn, flip = step
    block = power_block(ep_count)
    turns = ep_count // block
    return lax.rem(index // block + turns + sign * turn, turns) * block + lax.bitwise_xor(lax.rem(index, block), flip)


def tp_place():
    index = lax.axis_index("tp")
    return index // cores, lax.rem(index, cores)


def pack_kernel(order, near, experts, part, *refs):
    sources, dispatch, blocks = refs[:4], refs[4], refs[5:-7]
    targets, (place_at, weight_at, sems) = refs[-7:-3], refs[-3:]
    copies = [pltpu.make_async_copy(s, t, sems.at[i]) for i, (s, t) in enumerate(zip(sources, targets))]
    for copy in copies:
        copy.start()
    for copy in copies:
        copy.wait()
    tokens, routes, router, cotangent = targets
    ep_count = len(blocks)
    ep_index, tp_index = lax.axis_index("ep"), lax.axis_index("tp")
    rows, width = tokens.shape
    capacity = dispatch.shape[1]
    logits = dot(router[...], tokens[...], (1, 1))
    expert_at = iota((experts, rows), 0)
    hot = expert_at == routes[0:1, :]
    for k in range(1, routes.shape[0]):
        hot = hot | (expert_at == routes[k : k + 1, :])
    top = jnp.max(jnp.where(hot, logits, -jnp.inf), axis=0, keepdims=True)
    powers = jnp.where(hot, jnp.exp(jnp.where(hot, logits - top, 0.0)), 0.0)
    weights = powers / jnp.sum(powers, axis=0, keepdims=True)
    before = (iota((rows, rows), 0) < iota((rows, rows), 1)).astype(bf16)
    earlier = dot(jnp.where(hot, 1.0, 0.0).astype(bf16), before, (1, 0))
    place_at[:experts, :] = jnp.where(hot, earlier, -1.0)
    weight_at[...] = jnp.zeros_like(weight_at)
    weight_at[:experts, :] = weights
    full = weight_at[...].T
    high = full.astype(bf16).astype(f32)
    meta = (high + pltpu.roll(full - high, experts, 1)).astype(bf16)
    slots = iota((capacity, rows), 0).astype(f32)
    for index, (step, block) in enumerate(zip(order, blocks)):
        expert = moved_to(ep_index, step, ep_count, 1)
        chosen = slots == place_at[pl.ds(expert, 1), :]
        slot_weight = jnp.sum(jnp.where(chosen, weight_at[pl.ds(expert, 1), :], 0.0), axis=1, keepdims=True)
        pick = jnp.where(chosen, 1.0, 0.0).astype(bf16)
        dispatch[expert] = pick
        if index == 0:
            span, start = width, 0
        elif index < near:
            span = width // cores
            start = pl.multiple_of(lax.rem(tp_index, cores) * span, lanes)
        else:
            span = part
            start = pl.multiple_of(tp_index * span, lanes)
        block[:, :span] = dot(pick, tokens[:, pl.ds(start, span)], (1, 0)).astype(bf16)
        cots = dot(pick, cotangent[:, pl.ds(start, span)], (1, 0))
        block[:, span : 2 * span] = (slot_weight * cots).astype(bf16)
        block[:, 2 * span :] = dot(pick, meta, (1, 0)).astype(bf16)


def stage_kernel(source, target, sem):
    copy = pltpu.make_async_copy(source, target, sem)
    copy.start()
    copy.wait()


def put(rows, cots, piece, first, at, span):
    count = piece.shape[0]
    cols = pl.ds(at if isinstance(at, int) else pl.multiple_of(at, lanes), span)
    rows[first : first + count, cols] = piece[:, :span]
    cots[first : first + count, cols] = piece[:, span : 2 * span]


def expert_kernel(ys, experts, group, last, *refs):
    refs = list(refs)

    def take(count):
        taken = refs[:count]
        del refs[:count]
        return taken

    sent = take(3 if group == 0 else 2 * ys + 1)
    w_gate, w_up, w_down, router = take(4)
    if group:
        before = take(2 * ys)
        take(5)
    all_rows, all_cots, all_act, all_d_gate, all_d_up = take(5)
    outs = take(2 * ys)
    terms = [] if last else take(2 * ys)
    rows, cots, sem = refs
    count, width = cots.shape
    part = width // (cores * ys)
    y_index, core = tp_place()
    mine = pl.ds(group * count, count)
    act, d_gate, d_up = [r.at[mine] for r in (all_act, all_d_gate, all_d_up)]
    if group == 0:
        own, near, swapped = sent
        half = width // cores
        put(rows, cots, own, 0, 0, width)
        put(rows, cots, near, own.shape[0], core * half, half)
        put(rows, cots, swapped, own.shape[0], (1 - core) * half, half)
        meta = jnp.concatenate([own[:, 2 * width :], near[:, 2 * half :]], axis=0)
    else:
        meta = sent[2 * ys][...]
        for step in range(ys):
            y_from = lax.rem(y_index - step + ys, ys)
            put(rows, cots, sent[step], 0, (y_from * cores + core) * part, part)
            put(rows, cots, sent[ys + step], 0, (y_from * cores + 1 - core) * part, part)
    saves = [
        pltpu.make_async_copy(rows, all_rows.at[mine], sem.at[0]),
        pltpu.make_async_copy(cots, all_cots.at[mine], sem.at[1]),
    ]
    for save in saves:
        save.start()
    hidden = act.shape[1]
    tile = min(hidden, 256)
    share = jnp.zeros((count, 1), f32)
    for at in range(0, hidden, tile):
        cols = slice(at, at + tile)
        pre_gate = dot(rows[...], w_gate[:, cols], (1, 0))
        pre_up = dot(rows[...], w_up[:, cols], (1, 0))
        back = dot(cots[...], w_down[cols, :], (1, 1))
        gate_clamped = jnp.minimum(pre_gate, clamp_limit)
        up_one = jnp.clip(pre_up, -clamp_limit, clamp_limit) + 1.0
        sig = jax.nn.sigmoid(sig_slope * gate_clamped)
        gated = gate_clamped * sig
        made = (up_one * gated).astype(bf16)
        act[:, cols] = made
        share = share + jnp.sum(made.astype(f32) * back, axis=1, keepdims=True)
        slope = sig + sig_slope * gated * (1.0 - sig)
        d_gate[:, cols] = jnp.where(pre_gate < clamp_limit, back * up_one * slope, 0.0).astype(bf16)
        d_up[:, cols] = jnp.where(jnp.abs(pre_up) < clamp_limit, back * gated, 0.0).astype(bf16)
    wide = meta.shape[1]
    packed = meta.astype(f32)
    weights = packed + pltpu.roll(packed, wide - experts, 1)
    lane = iota((count, wide), 1)
    coef = jnp.where(lane == lax.axis_index("ep"), 1.0, 0.0) - weights
    d_logits = jnp.where(lane < experts, share * coef, 0.0)
    high = d_logits.astype(bf16)
    low = (d_logits - high.astype(f32)).astype(bf16)
    both = jnp.concatenate([high, low], axis=1)
    fill = jnp.zeros((wide - experts, part), f32)
    for step in reversed(range(ys)):
        y_to = lax.rem(y_index + step, ys)
        for index, c_to in ((ys + step, 1 - core), (step, core)):
            at = pl.multiple_of((y_to * cores + c_to) * part, lanes)
            value = dot(d_gate[...], w_gate[pl.ds(at, part), :], (1, 1))
            value = value + dot(d_up[...], w_up[pl.ds(at, part), :], (1, 1))
            side = jnp.concatenate([router[:, pl.ds(at, part)].astype(f32), fill], axis=0).astype(bf16)
            value = value + dot(both, jnp.concatenate([side, side], axis=0), (1, 0))
            outs[index][:count, :] = value.astype(bf16)
            term = dot(both, rows[:, pl.ds(at, part)], (0, 0))
            term = term[:experts] + term[wide : wide + experts]
            if group:
                term = term + before[index][...]
            if last:
                outs[index][count:, :] = term.astype(bf16)
            else:
                terms[index][...] = term
    for save in saves:
        save.wait()


def add_kernel(a, b, out):
    out[...] = (a[...].astype(f32) + b[...].astype(f32)).astype(bf16)


def return_kernel(order, capacity, *refs):
    parts, out = refs[:-1], refs[-1]
    ep_count = out.shape[0]
    ep_index = lax.axis_index("ep")
    ys = len(parts) // groups
    held = ep_count // groups
    for group in range(groups):
        total = parts[group * ys][...].astype(f32)
        for other in parts[group * ys + 1 : (group + 1) * ys]:
            total = total + other[...].astype(f32)
        total = total.astype(bf16)
        for at in range(held):
            to = moved_to(ep_index, order[group * held + at], ep_count, -1)
            out[to, :capacity, :] = total[at * capacity : (at + 1) * capacity]
    for to in range(ep_count):
        out[to, capacity:, :] = total[held * capacity :]


def grads_kernel(rows, cots, act, d_gate, d_up, gate, up, down, act_t):
    @pl.when(pl.program_id(0) == 0)
    def _():
        act_t[...] = act[...].T

    rows_t = rows[...].T
    gate[...] = dot(rows_t, d_gate[...], (1, 0))
    up[...] = dot(rows_t, d_up[...], (1, 0))
    down[...] = dot(act_t[...], cots[...], (1, 0))


def weight_grads(made, width, hidden, tile):
    count = made[0].shape[0]
    tall = pl.BlockSpec((tile, hidden), lambda i: (i, 0))
    some = pl.BlockSpec((count, tile), lambda i: (0, i))
    whole = pl.BlockSpec(memory_space=pltpu.VMEM)
    made = [pltpu.with_memory_space_constraint(m, pltpu.HBM) for m in made[:2]] + list(made[2:])
    return pl.pallas_call(
        grads_kernel,
        grid=(width // tile,),
        out_shape=[shaped((width, hidden), f32)] * 2 + [shaped((hidden, width), f32)],
        in_specs=[some, some, whole, whole, whole],
        out_specs=[tall, tall, pl.BlockSpec((hidden, tile), lambda i: (0, i))],
        scratch_shapes=[pltpu.VMEM((hidden, count), bf16)],
        compiler_params=pltpu.CompilerParams(vmem_limit_bytes=vmem_grant),
        cost_estimate=pl.CostEstimate(
            flops=6 * count * width * hidden, bytes_accessed=12 * width * hidden, transcendentals=0
        ),
    )(*made)


def combine_kernel(dispatch, back, grad_tokens, grad_router):
    ep_count, capacity = dispatch.shape[:2]
    total = dot(dispatch[0], back[0, :capacity], (0, 0))
    term = back[0, capacity:].astype(f32)
    for e in range(1, ep_count):
        total = total + dot(dispatch[e], back[e, :capacity], (0, 0))
        term = term + back[e, capacity:].astype(f32)
    grad_tokens[...] = total.astype(bf16)
    grad_router[...] = term


def on_device(tokens, routes, router, w_gate, w_up, w_down, cotangent):
    ep_count = lax.axis_size("ep")
    tp_count = lax.axis_size("tp")
    tok_rows, width = tokens.shape
    w_gate, w_up, w_down = w_gate[0], w_up[0], w_down[0]
    hidden = w_gate.shape[1]
    experts = router.shape[1]
    capacity = 3 * tok_rows * routes.shape[1] // (2 * experts)
    part, half = width // tp_count, width // cores
    ys = tp_count // cores
    held = ep_count // groups
    count = held * capacity
    wide = round_up(2 * experts, lanes)
    block = power_block(ep_count)
    order = [(turn, flip) for turn in range(ep_count // block) for flip in range(block)]
    to_core = [(i, i ^ 1) for i in range(tp_count)]

    def to_y(step):
        return [(i, (i + step * cores) % tp_count) for i in range(tp_count)]

    def to_ep(step):
        turn, flip = step
        return [(i, (i // block + turn) % (ep_count // block) * block + (i % block ^ flip)) for i in range(ep_count)]

    spans = [width] + [half] * (held - 1) + [part] * (ep_count - held)
    dispatch, *blocks = call(
        functools.partial(pack_kernel, order, held, experts, part),
        [shaped((ep_count, capacity, tok_rows), bf16)] + [shaped((capacity, 2 * s + wide), bf16) for s in spans],
        (tokens, routes.T, router.T, cotangent),
        2 * tok_rows * capacity * (2 * sum(spans) + wide * ep_count),
        [
            pltpu.VMEM(tokens.shape, bf16),
            pltpu.VMEM(routes.shape[::-1], i32),
            pltpu.VMEM(router.shape[::-1], bf16),
            pltpu.VMEM(cotangent.shape, bf16),
            pltpu.VMEM((wide, tok_rows), f32),
            pltpu.VMEM((wide, tok_rows), f32),
            pltpu.SemaphoreType.DMA((4,)),
        ],
        range(4),
    )
    (w_down,) = call(stage_kernel, [shaped(w_down.shape, bf16)], (w_down,), 10**9, [pltpu.SemaphoreType.DMA], (0,))
    got = [blocks[0]]
    for at in range(1, ep_count):
        got.append(lax.ppermute(blocks[at], "ep", to_ep(order[at])))
    made, terms, sums = (), (), []
    for group in range(groups):
        last = group == groups - 1
        here = got[group * held : (group + 1) * held]
        if group == 0:
            near = jnp.concatenate(here[1:], axis=0)
            sent = (here[0], near, lax.ppermute(near, "tp", to_core))
        else:
            mine = jnp.concatenate([g[:, : 2 * part] for g in here], axis=0)
            meta = jnp.concatenate([g[:, 2 * part :] for g in here], axis=0)
            own = [mine] + [lax.ppermute(mine, "tp", to_y(s)) for s in range(1, ys)]
            swapped = [lax.ppermute(own[0], "tp", to_core)]
            swapped += [lax.ppermute(o, "tp", to_core) for o in own[1:]]
            sent = (*own, *swapped, meta)
        outs = [pltpu.HBM((groups * count, width), bf16)] * 2 + [shaped((groups * count, hidden), bf16)] * 3
        outs = outs + [shaped((count + experts if last else count, part), bf16)] * (2 * ys)
        if not last:
            outs = outs + [shaped((experts, part), f32)] * (2 * ys)
        args = (*sent, w_gate, w_up, w_down, router.T, *terms)
        at = len(args)
        got_outs = call(
            functools.partial(expert_kernel, ys, experts, group, last),
            outs,
            (*args, *made),
            10 * count * width * hidden,
            [pltpu.VMEM((count, width), bf16), pltpu.VMEM((count, width), bf16), pltpu.SemaphoreType.DMA((2,))],
            (at, at + 1) if group else (),
            {at + i: i for i in range(5)} if group else None,
            (0, 1),
        )
        made = got_outs[:5]
        terms = got_outs[5 + 2 * ys :]
        keep, give = got_outs[5 : 5 + ys], got_outs[5 + ys : 5 + 2 * ys]
        pairs = [None] * ys
        for step in reversed(range(ys)):
            came = lax.ppermute(give[step], "tp", to_core)
            (pairs[step],) = call(add_kernel, [shaped(came.shape, bf16)], (keep[step], came), came.size)
        sums += [pairs[0]] + [lax.ppermute(pairs[s], "tp", to_y(s)) for s in range(1, ys)]
    (back,) = call(
        functools.partial(return_kernel, order, capacity),
        [shaped((ep_count, capacity + experts, part), bf16)],
        tuple(sums),
        count * part,
    )
    returned = lax.all_to_all(back, "ep", 0, 0, tiled=True)
    grad_gate, grad_up, grad_down = weight_grads(made, width, hidden, min(256, width))
    grad_tokens, grad_router = call(
        combine_kernel,
        [shaped((tok_rows, part), bf16), shaped((experts, part), f32)],
        (dispatch, returned),
        2 * tok_rows * part * capacity * ep_count,
    )
    return (grad_tokens, grad_router.T, grad_gate[None], grad_up[None], grad_down[None])


def solution(mesh):
    return jax.shard_map(
        on_device,
        mesh=mesh,
        in_specs=(
            P("ep", None),
            P("ep", None),
            P(),
            P("ep", None, "tp"),
            P("ep", None, "tp"),
            P("ep", "tp", None),
            P("ep", None),
        ),
        out_specs=(
            P("ep", "tp"),
            P("tp", None),
            P("ep", None, "tp"),
            P("ep", None, "tp"),
            P("ep", "tp", None),
        ),
        check_vma=False,
    )
```

profile of v0, /device:TPU:0, one launch (start us, length us, event | category | flops | bytes accessed | tf_op | source)
XLA Modules:
  0.0 89.6 jit_solution(14709266774234178666)
XLA Ops:
  0.6 2.4 %shard_map.110 = (bf16[8,48,128]{2,1,0:T(8,128)(2,1)S(1)}, bf16[48,4224]{1,0:T(8,128)(2,1)S(1)}, bf16[48,2176]{1,0:T(8,128)(2,1)S(1)}, bf16[48,2176]{1,0:T(8,128...) custom-call(bf16[128,2048]{1,0:T(8,128)(2,1)} %refs_0_.1, ...), custom_call_target="tpu_custom_call" | custom-call | flops 188743680 | bytes 2655232 | tf_op jit(solution)/shard_map/pallas_call | solution.py:31
  3.1 3.0 %collective-permute-start = (bf16[48,2176]{1,0:T(8,128)(2,1)S(1)}, bf16[48,2176]{1,0:T(8,128)(2,1)S(1)}, u32[]{:S(2)}, u32[]{:S(2)}) collective-permute-start(bf16[48,2176]{1,0:T(8,128)(2,1)S(1)} %get-tuple-element.43), channel_id=1, source_target_pairs={{0,4},{4,0},{8,12},{12,8},{16,20},{20,16},{24,28},{28,24},{1,5},{5... | collective-permute-start | bytes 626696 | tf_op jit(solution)/shard_map/ppermute | solution.py:332
  6.1 2.6 %collective-permute-start.7 = (bf16[48,1152]{1,0:T(8,128)(2,1)S(1)}, bf16[48,1152]{1,0:T(8,128)(2,1)S(1)}, u32[]{:S(2)}, u32[]{:S(2)}) collective-permute-start(bf16[48,1152]{1,0:T(8,128)(2,1)S(1)} %get-tuple-element.50), channel_id=1, source_target_pairs={{0,16},{4,20},{8,24},{12,28},{16,0},{20,4},{24,8},{28,12},{1,17},{... | collective-permute-start | bytes 331784 | tf_op jit(solution)/shard_map/ppermute | solution.py:332
  8.7 0.0 collective-permute-start.8
  8.7 3.9 %collective-permute-start.9 = (bf16[48,1152]{1,0:T(8,128)(2,1)S(1)}, bf16[48,1152]{1,0:T(8,128)(2,1)S(1)}, u32[]{:S(2)}, u32[]{:S(2)}) collective-permute-start(bf16[48,1152]{1,0:T(8,128)(2,1)S(1)} %get-tuple-element.52), channel_id=1, source_target_pairs={{0,24},{4,28},{8,16},{12,20},{16,8},{20,12},{24,0},{28,4},{1,25},{... | collective-permute-start | bytes 331784 | tf_op jit(solution)/shard_map/ppermute | solution.py:332
  12.6 1.1 %collective-permute-start.10 = (bf16[48,1152]{1,0:T(8,128)(2,1)S(1)}, bf16[48,1152]{1,0:T(8,128)(2,1)S(1)}, u32[]{:S(2)}, u32[]{:S(2)}) collective-permute-start(bf16[48,1152]{1,0:T(8,128)(2,1)S(1)} %get-tuple-element.53), channel_id=1, source_target_pairs={{0,28},{4,24},{8,20},{12,16},{16,12},{20,8},{24,4},{28,0},{1,29},{... | collective-permute-start | bytes 331784 | tf_op jit(solution)/shard_map/ppermute | solution.py:332
  13.8 8.4 %collective-permute-done.7 = bf16[48,1152]{1,0:T(8,128)(2,1)S(1)} collective-permute-done((bf16[48,1152]{1,0:T(8,128)(2,1)S(1)}, bf16[48,1152]{1,0:T(8,128)(2,1)S(1)}, u32[]{:S(2)}, u32[]{:S(2)}) %collective-permute-start.7) | collective-permute-done | bytes 110624 | tf_op jit(solution)/shard_map/ppermute | solution.py:332
  22.1 0.0 collective-permute-start.1
  22.1 2.2 %collective-permute-done.8 = bf16[48,1152]{1,0:T(8,128)(2,1)S(1)} collective-permute-done((bf16[48,1152]{1,0:T(8,128)(2,1)S(1)}, bf16[48,1152]{1,0:T(8,128)(2,1)S(1)}, u32[]{:S(2)}, u32[]{:S(2)}) %collective-permute-start.8) | collective-permute-done | bytes 110624 | tf_op jit(solution)/shard_map/ppermute | solution.py:332
  24.4 0.0 collective-permute-start.2
  24.4 0.0 collective-permute-done.9
  24.4 0.0 collective-permute-done.10
  24.5 0.0 collective-permute-done
  24.5 5.6 %collective-permute-done.1 = bf16[48,2176]{1,0:T(8,128)(2,1)S(1)} collective-permute-done((bf16[48,2176]{1,0:T(8,128)(2,1)S(1)}, bf16[48,2176]{1,0:T(8,128)(2,1)S(1)}, u32[]{:S(2)}, u32[]{:S(2)}) %collective-permute-start.1) | collective-permute-done | bytes 208928 | tf_op jit(solution)/shard_map/ppermute | solution.py:332
  30.1 2.3 %collective-permute-done.2 = bf16[48,2176]{1,0:T(8,128)(2,1)S(1)} collective-permute-done((bf16[48,2176]{1,0:T(8,128)(2,1)S(1)}, bf16[48,2176]{1,0:T(8,128)(2,1)S(1)}, u32[]{:S(2)}, u32[]{:S(2)}) %collective-permute-start.2) | collective-permute-done | bytes 208928 | tf_op jit(solution)/shard_map/ppermute | solution.py:332
  32.4 0.1 collective-permute-start.3
  32.5 1.6 %collective-permute-start.11 = (bf16[192,1024]{1,0:T(8,128)(2,1)S(1)}, bf16[192,1024]{1,0:T(8,128)(2,1)S(1)}, u32[]{:S(2)}, u32[]{:S(2)}) collective-permute-start(bf16[192,1024]{1,0:T(8,128)(2,1)S(1)} %pad_maximum_fusion.refs_0_), channel_id=1, source_target_pairs={{0,2},{1,3},{2,0},{3,1},{4,6},{5,7},{6,4},{7,5},{8,10},{9,11},{10,... | collective-permute-start | bytes 1179656 | tf_op jit(solution)/shard_map/ppermute | solution.py:343
  34.2 0.2 collective-permute-start.12
  34.4 9.7 %collective-permute-done.11.refs_1_ = bf16[192,1024]{1,0:T(8,128)(2,1)S(1)} collective-permute-done((bf16[192,1024]{1,0:T(8,128)(2,1)S(1)}, bf16[192,1024]{1,0:T(8,128)(2,1)S(1)}, u32[]{:S(2)}, u32[]{:S(2)}) %collective-permute-start.11) | collective-permute-done | bytes 393248 | tf_op jit(solution)/shard_map/ppermute | solution.py:343
  44.1 0.0 collective-permute-start.13
  44.1 0.0 copy-start
  44.1 0.0 copy-start.1
  44.1 0.0 copy-start.2
  44.1 1.8 %shard_map.111.refs_5_.refs_7_ = bf16[512,2048]{1,0:T(8,128)(2,1)S(1)} custom-call(bf16[512,2048]{1,0:T(8,128)(2,1)} %bitcast.16), custom_call_target="tpu_custom_call" | custom-call | flops 1000000000 | bytes 4194304 | tf_op jit(solution)/shard_map/pallas_call | solution.py:31
  46.0 0.0 collective-permute-done.3.refs_2_
  46.0 0.4 copy-done
  46.3 0.6 copy-done.1
  47.0 0.0 copy-done.2
  47.0 4.4 %shard_map.112 = (bf16[384,2048]{1,0:T(8,128)(2,1)}, bf16[384,2048]{1,0:T(8,128)(2,1)}, bf16[384,512]{1,0:T(8,128)(2,1)S(1)}, bf16[384,512]{1,0:T(8,128)(2,1)S(1...) custom-call(bf16[48,4224]{1,0:T(8,128)(2,1)S(1)} %get-tuple-element., ...), custom_call_target="tpu_custom_call" | custom-call | flops 2013265920 | bytes 13127680 | tf_op jit(solution)/shard_map/pallas_call | solution.py:31
  51.4 0.0 collective-permute-done.12.refs_2_
  51.4 0.0 collective-permute-done.13.refs_3_
  51.4 4.2 %shard_map.115 = (bf16[384,2048]{1,0:T(8,128)(2,1)}, bf16[384,2048]{1,0:T(8,128)(2,1)}, bf16[384,512]{1,0:T(8,128)(2,1)S(1)}, bf16[384,512]{1,0:T(8,128)(2,1)S(1...) custom-call(bf16[192,1024]{1,0:T(8,128)(2,1)S(1)} %pad_maximum_fusio, ...), custom_call_target="tpu_custom_call", output_to_operand_aliasing={{0}: (13, {}), {1}: (14, {}), {2}: (15, {}), {3}: (16, {}),... | custom-call | flops 2013265920 | bytes 17481728 | tf_op jit(solution)/shard_map/pallas_call | solution.py:31
  55.6 0.6 collective-permute-start.15
  56.2 0.1 collective-permute-start.5
  56.2 0.4 collective-permute-start.14
  56.7 0.6 collective-permute-done.15.b
  57.3 1.6 %collective-permute-start.16 = (bf16[200,512]{1,0:T(8,128)(2,1)S(1)}, bf16[200,512]{1,0:T(8,128)(2,1)S(1)}, u32[]{:S(2)}, u32[]{:S(2)}) collective-permute-start(bf16[200,512]{1,0:T(8,128)(2,1)S(1)} %shard_map.117), channel_id=1, source_target_pairs={{0,2},{1,3},{2,0},{3,1},{4,6},{5,7},{6,4},{7,5},{8,10},{9,11},{10,... | collective-permute-start | bytes 614408 | tf_op jit(solution)/shard_map/ppermute | solution.py:370
  58.9 0.1 collective-permute-start.4
  59.0 0.0 collective-permute-done.5.b
  59.1 0.5 collective-permute-start.6
  59.6 0.8 collective-permute-done.4.b
  60.4 0.0 collective-permute-done.14.b
  60.4 0.1 shard_map.116.refs_2_
  60.5 8.4 %collective-permute-done.6.refs_1_ = bf16[192,512]{1,0:T(8,128)(2,1)S(1)} collective-permute-done((bf16[192,512]{1,0:T(8,128)(2,1)S(1)}, bf16[192,512]{1,0:T(8,128)(2,1)S(1)}, u32[]{:S(2)}, u32[]{:S(2)}) %collective-permute-start.6) | collective-permute-done | bytes 196640 | tf_op jit(solution)/shard_map/ppermute | solution.py:370
  68.9 0.0 collective-permute-done.16.refs_3_
  68.9 0.9 shard_map.118
  69.8 5.8 %all-to-all-start = ((bf16[8,56,512]{2,1,0:T(8,128)(2,1)}), bf16[8,56,512]{2,1,0:T(8,128)(2,1)S(1)}, u32[]{:S(2)}, u32[]{:S(2)}) async-start(bf16[8,56,512]{2,1,0:T(8,128)(2,1)} %shard_map.118), calls=%async_computation | async-start | bytes 917504 | tf_op jit(solution)/shard_map/all_to_all | solution.py:377
  75.6 9.9 %shard_map.120 = (f32[2048,512]{1,0:T(8,128)}, f32[2048,512]{1,0:T(8,128)}, f32[512,2048]{1,0:T(8,128)}) custom-call(bf16[384,2048]{1,0:T(8,128)(2,1)} %get-tuple-element.69.rows, bf16[384,2048]{1,0:T(8,128)(2,1)} %get-tuple-element.70.cots, bf16[384,512]{1,0:T(8,128)(2,1)S(1)} %get-tuple-element.71.act, bf16[384,512]{1,0:T(8,128)(2,1)S(1)} %get-tuple-element.72.d_gate, ...), custom_call_target="tpu_custom_call" | custom-call | flops 2415919104 | bytes 12582912 | tf_op jit(solution)/shard_map/pallas_call | solution.py:263
  85.5 2.9 %all-to-all-done.back = bf16[8,56,512]{2,1,0:T(8,128)(2,1)S(1)} async-done(((bf16[8,56,512]{2,1,0:T(8,128)(2,1)}), bf16[8,56,512]{2,1,0:T(8,128)(2,1)S(1)}, u32[]{:S(2)}, u32[]{:S(2)}) %all-to-all-start) | async-done | bytes 458784 | tf_op jit(solution)/shard_map/all_to_all | solution.py:377
  88.4 1.1 %shard_map.119 = (bf16[128,512]{1,0:T(8,128)(2,1)}, f32[8,512]{1,0:T(8,128)}) custom-call(bf16[8,48,128]{2,1,0:T(8,128)(2,1)S(1)} %get-tuple-element.41.dispatch, bf16[8,56,512]{2,1,0:T(8,128)(2,1)S(1)} %all-to-all-done.back), custom_call_target="tpu_custom_call" | custom-call | flops 50331648 | bytes 696320 | tf_op jit(solution)/shard_map/pallas_call | solution.py:31
  (16 shorter events, 0.3 us)
Async XLA Ops:
  3.1 21.4 %collective-permute-start = (bf16[48,2176]{1,0:T(8,128)(2,1)S(1)}, bf16[48,2176]{1,0:T(8,128)(2,1)S(1)}, u32[]{:S(2)}, u32[]{:S(2)}) collective-permute-start(bf16[48,2176]{1,0:T(8,128)(2,1)S(1)} %get-tuple-element.43), channel_id=1, source_target_pairs={{0,4},{4,0},{8,12},{12,8},{16,20},{20,16},{24,28},{28,24},{1,5},{5... | collective-permute-start | bytes 626696 | tf_op jit(solution)/shard_map/ppermute | solution.py:332
  6.1 16.0 %collective-permute-start.7 = (bf16[48,1152]{1,0:T(8,128)(2,1)S(1)}, bf16[48,1152]{1,0:T(8,128)(2,1)S(1)}, u32[]{:S(2)}, u32[]{:S(2)}) collective-permute-start(bf16[48,1152]{1,0:T(8,128)(2,1)S(1)} %get-tuple-element.50), channel_id=1, source_target_pairs={{0,16},{4,20},{8,24},{12,28},{16,0},{20,4},{24,8},{28,12},{1,17},{... | collective-permute-start | bytes 331784 | tf_op jit(solution)/shard_map/ppermute | solution.py:332
  8.7 15.7 %collective-permute-start.8 = (bf16[48,1152]{1,0:T(8,128)(2,1)S(1)}, bf16[48,1152]{1,0:T(8,128)(2,1)S(1)}, u32[]{:S(2)}, u32[]{:S(2)}) collective-permute-start(bf16[48,1152]{1,0:T(8,128)(2,1)S(1)} %get-tuple-element.51), channel_id=1, source_target_pairs={{0,20},{4,16},{8,28},{12,24},{16,4},{20,0},{24,12},{28,8},{1,21},{... | collective-permute-start | bytes 331784 | tf_op jit(solution)/shard_map/ppermute | solution.py:332
  8.7 15.7 %collective-permute-start.9 = (bf16[48,1152]{1,0:T(8,128)(2,1)S(1)}, bf16[48,1152]{1,0:T(8,128)(2,1)S(1)}, u32[]{:S(2)}, u32[]{:S(2)}) collective-permute-start(bf16[48,1152]{1,0:T(8,128)(2,1)S(1)} %get-tuple-element.52), channel_id=1, source_target_pairs={{0,24},{4,28},{8,16},{12,20},{16,8},{20,12},{24,0},{28,4},{1,25},{... | collective-permute-start | bytes 331784 | tf_op jit(solution)/shard_map/ppermute | solution.py:332
  12.6 11.8 %collective-permute-start.10 = (bf16[48,1152]{1,0:T(8,128)(2,1)S(1)}, bf16[48,1152]{1,0:T(8,128)(2,1)S(1)}, u32[]{:S(2)}, u32[]{:S(2)}) collective-permute-start(bf16[48,1152]{1,0:T(8,128)(2,1)S(1)} %get-tuple-element.53), channel_id=1, source_target_pairs={{0,28},{4,24},{8,20},{12,16},{16,12},{20,8},{24,4},{28,0},{1,29},{... | collective-permute-start | bytes 331784 | tf_op jit(solution)/shard_map/ppermute | solution.py:332
  22.1 8.0 %collective-permute-start.1 = (bf16[48,2176]{1,0:T(8,128)(2,1)S(1)}, bf16[48,2176]{1,0:T(8,128)(2,1)S(1)}, u32[]{:S(2)}, u32[]{:S(2)}) collective-permute-start(bf16[48,2176]{1,0:T(8,128)(2,1)S(1)} %get-tuple-element.44), channel_id=1, source_target_pairs={{0,8},{4,12},{8,0},{12,4},{16,24},{20,28},{24,16},{28,20},{1,9},{5... | collective-permute-start | bytes 626696 | tf_op jit(solution)/shard_map/ppermute | solution.py:332
  24.4 8.0 %collective-permute-start.2 = (bf16[48,2176]{1,0:T(8,128)(2,1)S(1)}, bf16[48,2176]{1,0:T(8,128)(2,1)S(1)}, u32[]{:S(2)}, u32[]{:S(2)}) collective-permute-start(bf16[48,2176]{1,0:T(8,128)(2,1)S(1)} %get-tuple-element.45), channel_id=1, source_target_pairs={{0,12},{4,8},{8,4},{12,0},{16,28},{20,24},{24,20},{28,16},{1,13},{... | collective-permute-start | bytes 626696 | tf_op jit(solution)/shard_map/ppermute | solution.py:332
  32.4 13.5 %collective-permute-start.3 = (bf16[144,2176]{1,0:T(8,128)(2,1)S(1)}, bf16[144,2176]{1,0:T(8,128)(2,1)S(1)}, u32[]{:S(2)}, u32[]{:S(2)}) collective-permute-start(bf16[144,2176]{1,0:T(8,128)(2,1)S(1)} %constant_dynamic-update-slice_fusion.refs_1_), channel_id=1, source_target_pairs={{0,1},{1,0},{2,3},{3,2},{4,5},{5,4},{6,7},{7,6},{8,9},{9,8},{10,11... | collective-permute-start | bytes 1880072 | tf_op jit(solution)/shard_map/ppermute | solution.py:339
  32.5 11.6 %collective-permute-start.11 = (bf16[192,1024]{1,0:T(8,128)(2,1)S(1)}, bf16[192,1024]{1,0:T(8,128)(2,1)S(1)}, u32[]{:S(2)}, u32[]{:S(2)}) collective-permute-start(bf16[192,1024]{1,0:T(8,128)(2,1)S(1)} %pad_maximum_fusion.refs_0_), channel_id=1, source_target_pairs={{0,2},{1,3},{2,0},{3,1},{4,6},{5,7},{6,4},{7,5},{8,10},{9,11},{10,... | collective-permute-start | bytes 1179656 | tf_op jit(solution)/shard_map/ppermute | solution.py:343
  34.2 17.2 %collective-permute-start.12 = (bf16[192,1024]{1,0:T(8,128)(2,1)S(1)}, bf16[192,1024]{1,0:T(8,128)(2,1)S(1)}, u32[]{:S(2)}, u32[]{:S(2)}) collective-permute-start(bf16[192,1024]{1,0:T(8,128)(2,1)S(1)} %pad_maximum_fusion.refs_0_), channel_id=1, source_target_pairs={{0,1},{1,0},{2,3},{3,2},{4,5},{5,4},{6,7},{7,6},{8,9},{9,8},{10,11... | collective-permute-start | bytes 1179656 | tf_op jit(solution)/shard_map/ppermute | solution.py:344
  44.1 7.3 %collective-permute-start.13 = (bf16[192,1024]{1,0:T(8,128)(2,1)S(1)}, bf16[192,1024]{1,0:T(8,128)(2,1)S(1)}, u32[]{:S(2)}, u32[]{:S(2)}) collective-permute-start(bf16[192,1024]{1,0:T(8,128)(2,1)S(1)} %collective-permute-done.11.refs_1_), channel_id=1, source_target_pairs={{0,1},{1,0},{2,3},{3,2},{4,5},{5,4},{6,7},{7,6},{8,9},{9,8},{10,11... | collective-permute-start | bytes 1179656 | tf_op jit(solution)/shard_map/ppermute | solution.py:345
  44.1 2.2 %copy-start = (bf16[1,2048,512]{2,1,0:T(8,128)(2,1)S(1)}, bf16[1,2048,512]{2,1,0:T(8,128)(2,1)}, u32[]{:S(2)}) copy-start(bf16[1,2048,512]{2,1,0:T(8,128)(2,1)} %param.10) | copy-start | bytes 6291460
  44.1 2.9 %copy-start.1 = (bf16[1,2048,512]{2,1,0:T(8,128)(2,1)S(1)}, bf16[1,2048,512]{2,1,0:T(8,128)(2,1)}, u32[]{:S(2)}) copy-start(bf16[1,2048,512]{2,1,0:T(8,128)(2,1)} %param.11) | copy-start | bytes 6291460
  44.1 2.9 %copy-start.2 = (bf16[2048,8]{0,1:T(8,128)(2,1)S(1)}, bf16[2048,8]{0,1:T(8,128)(2,1)}, u32[]{:S(2)}) copy-start(bf16[2048,8]{0,1:T(8,128)(2,1)} %param.9) | copy-start | bytes 98308
  55.6 1.7 %collective-permute-start.15 = (bf16[200,512]{1,0:T(8,128)(2,1)S(1)}, bf16[200,512]{1,0:T(8,128)(2,1)S(1)}, u32[]{:S(2)}, u32[]{:S(2)}) collective-permute-start(bf16[200,512]{1,0:T(8,128)(2,1)S(1)} %get-tuple-element.66), channel_id=1, source_target_pairs={{0,1},{1,0},{2,3},{3,2},{4,5},{5,4},{6,7},{7,6},{8,9},{9,8},{10,11... | collective-permute-start | bytes 614408 | tf_op jit(solution)/shard_map/ppermute | solution.py:368
  56.2 2.9 %collective-permute-start.5 = (bf16[192,512]{1,0:T(8,128)(2,1)S(1)}, bf16[192,512]{1,0:T(8,128)(2,1)S(1)}, u32[]{:S(2)}, u32[]{:S(2)}) collective-permute-start(bf16[192,512]{1,0:T(8,128)(2,1)S(1)} %get-tuple-element.49), channel_id=1, source_target_pairs={{0,1},{1,0},{2,3},{3,2},{4,5},{5,4},{6,7},{7,6},{8,9},{9,8},{10,11... | collective-permute-start | bytes 589832 | tf_op jit(solution)/shard_map/ppermute | solution.py:368
  56.2 4.2 %collective-permute-start.14 = (bf16[200,512]{1,0:T(8,128)(2,1)S(1)}, bf16[200,512]{1,0:T(8,128)(2,1)S(1)}, u32[]{:S(2)}, u32[]{:S(2)}) collective-permute-start(bf16[200,512]{1,0:T(8,128)(2,1)S(1)} %get-tuple-element.64), channel_id=1, source_target_pairs={{0,1},{1,0},{2,3},{3,2},{4,5},{5,4},{6,7},{7,6},{8,9},{9,8},{10,11... | collective-permute-start | bytes 614408 | tf_op jit(solution)/shard_map/ppermute | solution.py:368
  57.3 11.6 %collective-permute-start.16 = (bf16[200,512]{1,0:T(8,128)(2,1)S(1)}, bf16[200,512]{1,0:T(8,128)(2,1)S(1)}, u32[]{:S(2)}, u32[]{:S(2)}) collective-permute-start(bf16[200,512]{1,0:T(8,128)(2,1)S(1)} %shard_map.117), channel_id=1, source_target_pairs={{0,2},{1,3},{2,0},{3,1},{4,6},{5,7},{6,4},{7,5},{8,10},{9,11},{10,... | collective-permute-start | bytes 614408 | tf_op jit(solution)/shard_map/ppermute | solution.py:370
  58.9 1.4 %collective-permute-start.4 = (bf16[192,512]{1,0:T(8,128)(2,1)S(1)}, bf16[192,512]{1,0:T(8,128)(2,1)S(1)}, u32[]{:S(2)}, u32[]{:S(2)}) collective-permute-start(bf16[192,512]{1,0:T(8,128)(2,1)S(1)} %get-tuple-element.47), channel_id=1, source_target_pairs={{0,1},{1,0},{2,3},{3,2},{4,5},{5,4},{6,7},{7,6},{8,9},{9,8},{10,11... | collective-permute-start | bytes 589832 | tf_op jit(solution)/shard_map/ppermute | solution.py:368
  59.1 9.9 %collective-permute-start.6 = (bf16[192,512]{1,0:T(8,128)(2,1)S(1)}, bf16[192,512]{1,0:T(8,128)(2,1)S(1)}, u32[]{:S(2)}, u32[]{:S(2)}) collective-permute-start(bf16[192,512]{1,0:T(8,128)(2,1)S(1)} %shard_map.114), channel_id=1, source_target_pairs={{0,2},{1,3},{2,0},{3,1},{4,6},{5,7},{6,4},{7,5},{8,10},{9,11},{10,... | collective-permute-start | bytes 589832 | tf_op jit(solution)/shard_map/ppermute | solution.py:370
  69.8 18.6 %all-to-all-start = ((bf16[8,56,512]{2,1,0:T(8,128)(2,1)}), bf16[8,56,512]{2,1,0:T(8,128)(2,1)S(1)}, u32[]{:S(2)}, u32[]{:S(2)}) async-start(bf16[8,56,512]{2,1,0:T(8,128)(2,1)} %shard_map.118), calls=%async_computation | async-start | bytes 917504 | tf_op jit(solution)/shard_map/all_to_all | solution.py:377
where the time goes:
time: 90 us; the launch traced here: 89.6 us
  waiting for transfers between devices  41 us (46%)
  Pallas kernels  24.8 us (28%)
  starting transfers between devices  21.8 us (24%)
  local copies, waits for them, and re-layouts  1.12 us (1%)
    ppermute x7, waiting for transfers between devices, on_device(): got.append(lax.ppermute(blocks[at], 'ep', to_ep(order[at])))  18.5 us
    pallas_call x10, Pallas kernels, call(): pl.pallas_call(kernel, out_shape=outs, in_specs=[hbm if i in in_hbm else...  14.9 us
    ppermute x7, starting transfers between devices, on_device(): got.append(lax.ppermute(blocks[at], 'ep', to_ep(order[at])))  10.7 us
    pallas_call x1, Pallas kernels, weight_grads(): pl.pallas_call(grads_kernel, grid=(width // tile,), out_shape=[shaped((wi...  9.89 us
    ppermute x1, waiting for transfers between devices, on_device(): own = [mine] + [lax.ppermute(mine, 'tp', to_y(s)) for s in range(1, ys)]  9.74 us
    ppermute x2, waiting for transfers between devices, on_device(): lax.ppermute(pairs[s], 'tp', to_y(s))  8.44 us
    all_to_all x1, starting transfers between devices, on_device(): returned = lax.all_to_all(back, 'ep', 0, 0, tiled=True)  5.83 us
    all_to_all x1, waiting for transfers between devices, on_device(): returned = lax.all_to_all(back, 'ep', 0, 0, tiled=True)  2.92 us
  transfers between devices with their start and end apart: 18, of which 9 were waited for; matrix products, arithmetic and copies ran while one was open for 0% of the time, Pallas kernels for 18%

commit v1 on v0

--- a/solution.py
+++ b/solution.py
@@ -74,7 +74,7 @@
     copies = [pltpu.make_async_copy(s, t, sems.at[i]) for i, (s, t) in enumerate(zip(sources, targets))]
     for copy in copies:
         copy.start()
-    for copy in copies:
+    for copy in copies[:-1]:
         copy.wait()
     tokens, routes, router, cotangent = targets
     ep_count = len(blocks)
@@ -97,12 +97,16 @@
     full = weight_at[...].T
     high = full.astype(bf16).astype(f32)
     meta = (high + pltpu.roll(full - high, experts, 1)).astype(bf16)
-    slots = iota((capacity, rows), 0).astype(f32)
+    low = weights - weights.astype(bf16).astype(f32)
+    both_t = jnp.concatenate([weights.astype(bf16).astype(f32), low], axis=0).astype(bf16)
+    slots = iota((lanes, rows), 0).astype(f32)
+    copies[-1].wait()
     for index, (step, block) in enumerate(zip(order, blocks)):
         expert = moved_to(ep_index, step, ep_count, 1)
         chosen = slots == place_at[pl.ds(expert, 1), :]
         slot_weight = jnp.sum(jnp.where(chosen, weight_at[pl.ds(expert, 1), :], 0.0), axis=1, keepdims=True)
-        pick = jnp.where(chosen, 1.0, 0.0).astype(bf16)
+        all_pick = jnp.where(chosen, 1.0, 0.0).astype(bf16)
+        pick, slot_weight = all_pick[:capacity], slot_weight[:capacity]
         dispatch[expert] = pick
         if index == 0:
             span, start = width, 0
@@ -112,10 +116,19 @@
         else:
             span = part
             start = pl.multiple_of(tp_index * span, lanes)
-        block[:, :span] = dot(pick, tokens[:, pl.ds(start, span)], (1, 0)).astype(bf16)
-        cots = dot(pick, cotangent[:, pl.ds(start, span)], (1, 0))
-        block[:, span : 2 * span] = (slot_weight * cots).astype(bf16)
-        block[:, 2 * span :] = dot(pick, meta, (1, 0)).astype(bf16)
+        toks = dot(pick, tokens[:, pl.ds(start, span)], (1, 0)).astype(bf16)
+        cots = (slot_weight * dot(pick, cotangent[:, pl.ds(start, span)], (1, 0))).astype(bf16)
+        if index < near:
+            block[:, :span] = toks
+            block[:, span : 2 * span] = cots
+            block[:, 2 * span :] = dot(pick, meta, (1, 0)).astype(bf16)
+            continue
+        tall = span // lanes
+        for at in range(tall):
+            cols = slice(at * lanes, (at + 1) * lanes)
+            block[at * capacity : (at + 1) * capacity, :] = toks[:, cols]
+            block[(tall + at) * capacity : (tall + at + 1) * capacity, :] = cots[:, cols]
+        block[2 * tall * capacity :, :] = dot(both_t, all_pick, (1, 1)).astype(bf16)
 
 
 def stage_kernel(source, target, sem):
@@ -129,6 +142,19 @@
     cols = pl.ds(at if isinstance(at, int) else pl.multiple_of(at, lanes), span)
     rows[first : first + count, cols] = piece[:, :span]
     cots[first : first + count, cols] = piece[:, span : 2 * span]
+
+
+def put_stacked(rows, cots, piece, blocks, at, span):
+    tall = span // lanes
+    high = piece.shape[0] // (2 * tall * blocks)
+    for block in range(blocks):
+        to = slice(block * high, (block + 1) * high)
+        for col in range(tall):
+            cols = pl.ds(pl.multiple_of(at + col * lanes, lanes), lanes)
+            first = (2 * tall * block + col) * high
+            rows[to, cols] = piece[first : first + high, :]
+            first = first + tall * high
+            cots[to, cols] = piece[first : first + high, :]
 
 
 def expert_kernel(ys, experts, group, last, *refs):
@@ -159,13 +185,22 @@
         put(rows, cots, own, 0, 0, width)
         put(rows, cots, near, own.shape[0], core * half, half)
         put(rows, cots, swapped, own.shape[0], (1 - core) * half, half)
-        meta = jnp.concatenate([own[:, 2 * width :], near[:, 2 * half :]], axis=0)
+        packed = jnp.concatenate([own[:, 2 * width :], near[:, 2 * half :]], axis=0).astype(f32)
+        weights = packed + pltpu.roll(packed, packed.shape[1] - experts, 1)
     else:
-        meta = sent[2 * ys][...]
+        packed = sent[2 * ys][...].astype(f32)
+        blocks = packed.shape[0] // (2 * experts)
         for step in range(ys):
             y_from = lax.rem(y_index - step + ys, ys)
-            put(rows, cots, sent[step], 0, (y_from * cores + core) * part, part)
-            put(rows, cots, sent[ys + step], 0, (y_from * cores + 1 - core) * part, part)
+            put_stacked(rows, cots, sent[step], blocks, (y_from * cores + core) * part, part)
+            put_stacked(rows, cots, sent[ys + step], blocks, (y_from * cores + 1 - core) * part, part)
+        fill = jnp.zeros((lanes - experts, lanes), f32)
+        weights = []
+        for block in range(blocks):
+            high = packed[2 * experts * block : 2 * experts * block + experts]
+            low = packed[2 * experts * block + experts : 2 * experts * (block + 1)]
+            weights.append(jnp.concatenate([high + low, fill], axis=0).T[: count // blocks])
+        weights = jnp.concatenate(weights, axis=0)
     saves = [
         pltpu.make_async_copy(rows, all_rows.at[mine], sem.at[0]),
         pltpu.make_async_copy(cots, all_cots.at[mine], sem.at[1]),
@@ -190,9 +225,7 @@
         slope = sig + sig_slope * gated * (1.0 - sig)
         d_gate[:, cols] = jnp.where(pre_gate < clamp_limit, back * up_one * slope, 0.0).astype(bf16)
         d_up[:, cols] = jnp.where(jnp.abs(pre_up) < clamp_limit, back * gated, 0.0).astype(bf16)
-    wide = meta.shape[1]
-    packed = meta.astype(f32)
-    weights = packed + pltpu.roll(packed, wide - experts, 1)
+    wide = weights.shape[1]
     lane = iota((count, wide), 1)
     coef = jnp.where(lane == lax.axis_index("ep"), 1.0, 0.0) - weights
     d_logits = jnp.where(lane < experts, share * coef, 0.0)
@@ -243,35 +276,30 @@
         out[to, capacity:, :] = total[held * capacity :]
 
 
-def grads_kernel(rows, cots, act, d_gate, d_up, gate, up, down, act_t):
-    @pl.when(pl.program_id(0) == 0)
-    def _():
-        act_t[...] = act[...].T
-
-    rows_t = rows[...].T
-    gate[...] = dot(rows_t, d_gate[...], (1, 0))
-    up[...] = dot(rows_t, d_up[...], (1, 0))
-    down[...] = dot(act_t[...], cots[...], (1, 0))
-
-
-def weight_grads(made, width, hidden, tile):
-    count = made[0].shape[0]
-    tall = pl.BlockSpec((tile, hidden), lambda i: (i, 0))
-    some = pl.BlockSpec((count, tile), lambda i: (0, i))
-    whole = pl.BlockSpec(memory_space=pltpu.VMEM)
-    made = [pltpu.with_memory_space_constraint(m, pltpu.HBM) for m in made[:2]] + list(made[2:])
+def tall_kernel(rows, d_gate, d_up, gate, up):
+    gate[...] = dot(rows[...], d_gate[...], (0, 0))
+    up[...] = dot(rows[...], d_up[...], (0, 0))
+
+
+def flat_kernel(cots, act, down):
+    down[...] = dot(act[...], cots[...], (0, 0))
+
+
+def weight_grads(kernel, spread, held, out_shape, out_spec, tile):
+    count, width = spread.shape
     return pl.pallas_call(
-        grads_kernel,
+        kernel,
         grid=(width // tile,),
-        out_shape=[shaped((width, hidden), f32)] * 2 + [shaped((hidden, width), f32)],
-        in_specs=[some, some, whole, whole, whole],
-        out_specs=[tall, tall, pl.BlockSpec((hidden, tile), lambda i: (0, i))],
-        scratch_shapes=[pltpu.VMEM((hidden, count), bf16)],
+        out_shape=out_shape,
+        in_specs=[pl.BlockSpec((count, tile), lambda i: (0, i))] + [pl.BlockSpec(memory_space=pltpu.VMEM)] * len(held),
+        out_specs=out_spec,
         compiler_params=pltpu.CompilerParams(vmem_limit_bytes=vmem_grant),
         cost_estimate=pl.CostEstimate(
-            flops=6 * count * width * hidden, bytes_accessed=12 * width * hidden, transcendentals=0
+            flops=2 * count * sum(math.prod(o.shape) for o in out_shape),
+            bytes_accessed=4 * sum(math.prod(o.shape) for o in out_shape),
+            transcendentals=0,
         ),
-    )(*made)
+    )(pltpu.with_memory_space_constraint(spread, pltpu.HBM), *held)
 
 
 def combine_kernel(dispatch, back, grad_tokens, grad_router):
@@ -309,12 +337,13 @@
         turn, flip = step
         return [(i, (i // block + turn) % (ep_count // block) * block + (i % block ^ flip)) for i in range(ep_count)]
 
-    spans = [width] + [half] * (held - 1) + [part] * (ep_count - held)
+    shapes = [(capacity, 2 * width + wide)] + [(capacity, 2 * half + wide)] * (held - 1)
+    shapes += [(2 * part // lanes * capacity + 2 * experts, lanes)] * (ep_count - held)
     dispatch, *blocks = call(
         functools.partial(pack_kernel, order, held, experts, part),
-        [shaped((ep_count, capacity, tok_rows), bf16)] + [shaped((capacity, 2 * s + wide), bf16) for s in spans],
+        [shaped((ep_count, capacity, tok_rows), bf16)] + [shaped(s, bf16) for s in shapes],
         (tokens, routes.T, router.T, cotangent),
-        2 * tok_rows * capacity * (2 * sum(spans) + wide * ep_count),
+        2 * tok_rows * sum(math.prod(s) for s in shapes),
         [
             pltpu.VMEM(tokens.shape, bf16),
             pltpu.VMEM(routes.shape[::-1], i32),
@@ -338,8 +367,8 @@
             near = jnp.concatenate(here[1:], axis=0)
             sent = (here[0], near, lax.ppermute(near, "tp", to_core))
         else:
-            mine = jnp.concatenate([g[:, : 2 * part] for g in here], axis=0)
-            meta = jnp.concatenate([g[:, 2 * part :] for g in here], axis=0)
+            mine = jnp.concatenate([g[: -2 * experts] for g in here], axis=0)
+            meta = jnp.concatenate([g[-2 * experts :] for g in here], axis=0)
             own = [mine] + [lax.ppermute(mine, "tp", to_y(s)) for s in range(1, ys)]
             swapped = [lax.ppermute(own[0], "tp", to_core)]
             swapped += [lax.ppermute(o, "tp", to_core) for o in own[1:]]
@@ -375,7 +404,16 @@
         count * part,
     )
     returned = lax.all_to_all(back, "ep", 0, 0, tiled=True)
-    grad_gate, grad_up, grad_down = weight_grads(made, width, hidden, min(256, width))
+    rows, cots, act, d_gate, d_up = made
+    tile = min(512, width)
+    (grad_down,) = weight_grads(
+        flat_kernel, cots, (act,), [shaped((hidden, width), f32)],
+        [pl.BlockSpec((hidden, tile), lambda i: (0, i))], tile,
+    )
+    grad_gate, grad_up = weight_grads(
+        tall_kernel, rows, (d_gate, d_up), [shaped((width, hidden), f32)] * 2,
+        [pl.BlockSpec((tile, hidden), lambda i: (i, 0))] * 2, tile,
+    )
     grad_tokens, grad_router = call(
         combine_kernel,
         [shaped((tok_rows, part), bf16), shaped((experts, part), f32)],

time: 90 us -> 90 us (level)
  waiting for transfers between devices: 41 us -> 31.2 us
  starting transfers between devices: 21.8 us -> 30.4 us
  Pallas kernels: 24.8 us -> 26 us
    ppermute x7, starting transfers between devices: 10.7 us -> 21.7 us  [on_device(): got.append(lax.ppermute(blocks[at], 'ep', to_ep(order[at])))]
    ppermute x7, waiting for transfers between devices: 18.5 us -> 9.4 us  [on_device(): got.append(lax.ppermute(blocks[at], 'ep', to_ep(order[at])))]
    all_to_all x1, starting transfers between devices: 5.83 us -> 3.47 us  [on_device(): returned = lax.all_to_all(back, 'ep', 0, 0, tiled=True)]
    pallas_call x1 -> x2, Pallas kernels: 9.89 us -> 10.7 us  [weight_grads(): pl.pallas_call(kernel, grid=(width // tile,), out_shape=out_shape, in_spe...]
  transfers between devices with their start and end apart: 18 -> 18, of which waited for: 9 -> 9; matrix products, arithmetic and copies ran while one was open for 0% -> 0% of each run, Pallas kernels for 18% -> 19%
where the time goes in v1:
time: 90 us; the launch traced here: 89.6 us
  waiting for transfers between devices  31.2 us (35%)
  starting transfers between devices  30.4 us (34%)
  Pallas kernels  26 us (29%)
  local copies, waits for them, and re-layouts  1.12 us (1%)
    ppermute x7, starting transfers between devices, on_device(): got.append(lax.ppermute(blocks[at], 'ep', to_ep(order[at])))  21.7 us
    pallas_call x10, Pallas kernels, call(): pl.pallas_call(kernel, out_shape=outs, in_specs=[hbm if i in in_hbm else...  15.3 us
    pallas_call x2, Pallas kernels, weight_grads(): pl.pallas_call(kernel, grid=(width // tile,), out_shape=out_shape, in_spe...  10.7 us
    ppermute x1, waiting for transfers between devices, on_device(): own = [mine] + [lax.ppermute(mine, 'tp', to_y(s)) for s in range(1, ys)]  9.78 us
    ppermute x7, waiting for transfers between devices, on_device(): got.append(lax.ppermute(blocks[at], 'ep', to_ep(order[at])))  9.4 us
    ppermute x2, waiting for transfers between devices, on_device(): lax.ppermute(pairs[s], 'tp', to_y(s))  8.47 us
    all_to_all x1, starting transfers between devices, on_device(): returned = lax.all_to_all(back, 'ep', 0, 0, tiled=True)  3.47 us
    all_to_all x1, waiting for transfers between devices, on_device(): returned = lax.all_to_all(back, 'ep', 0, 0, tiled=True)  2.28 us
  transfers between devices with their start and end apart: 18, of which 9 were waited for; matrix products, arithmetic and copies ran while one was open for 0% of the time, Pallas kernels for 19%

profile of v1, /device:TPU:0, one launch (start us, length us, event | category | flops | bytes accessed | tf_op | source)
XLA Modules:
  0.0 89.6 jit_solution(1276210135534126591)
XLA Ops:
  0.6 2.5 %shard_map.110 = (bf16[8,48,128]{2,1,0:T(8,128)(2,1)S(1)}, bf16[48,4224]{1,0:T(8,128)(2,1)S(1)}, bf16[48,2176]{1,0:T(8,128)(2,1)S(1)}, bf16[48,2176]{1,0:T(8,128...) custom-call(bf16[128,2048]{1,0:T(8,128)(2,1)} %refs_0_.1, ...), custom_call_target="tpu_custom_call" | custom-call | flops 184549376 | bytes 2622464 | tf_op jit(solution)/shard_map/pallas_call | solution.py:31
  3.2 3.0 %collective-permute-start = (bf16[48,2176]{1,0:T(8,128)(2,1)S(1)}, bf16[48,2176]{1,0:T(8,128)(2,1)S(1)}, u32[]{:S(2)}, u32[]{:S(2)}) collective-permute-start(bf16[48,2176]{1,0:T(8,128)(2,1)S(1)} %get-tuple-element.42), channel_id=1, source_target_pairs={{0,4},{4,0},{8,12},{12,8},{16,20},{20,16},{24,28},{28,24},{1,5},{5... | collective-permute-start | bytes 626696 | tf_op jit(solution)/shard_map/ppermute | solution.py:361
  6.2 3.6 %collective-permute-start.10 = (bf16[400,128]{1,0:T(8,128)(2,1)S(1)}, bf16[400,128]{1,0:T(8,128)(2,1)S(1)}, u32[]{:S(2)}, u32[]{:S(2)}) collective-permute-start(bf16[400,128]{1,0:T(8,128)(2,1)S(1)} %get-tuple-element.52), channel_id=1, source_target_pairs={{0,28},{4,24},{8,20},{12,16},{16,12},{20,8},{24,4},{28,0},{1,29},{... | collective-permute-start | bytes 307208 | tf_op jit(solution)/shard_map/ppermute | solution.py:361
  9.8 0.0 collective-permute-start.9
  9.8 1.9 %collective-permute-start.8 = (bf16[400,128]{1,0:T(8,128)(2,1)S(1)}, bf16[400,128]{1,0:T(8,128)(2,1)S(1)}, u32[]{:S(2)}, u32[]{:S(2)}) collective-permute-start(bf16[400,128]{1,0:T(8,128)(2,1)S(1)} %get-tuple-element.50), channel_id=1, source_target_pairs={{0,20},{4,16},{8,28},{12,24},{16,4},{20,0},{24,12},{28,8},{1,21},{... | collective-permute-start | bytes 307208 | tf_op jit(solution)/shard_map/ppermute | solution.py:361
  11.7 2.1 %collective-permute-start.7 = (bf16[400,128]{1,0:T(8,128)(2,1)S(1)}, bf16[400,128]{1,0:T(8,128)(2,1)S(1)}, u32[]{:S(2)}, u32[]{:S(2)}) collective-permute-start(bf16[400,128]{1,0:T(8,128)(2,1)S(1)} %get-tuple-element.49), channel_id=1, source_target_pairs={{0,16},{4,20},{8,24},{12,28},{16,0},{20,4},{24,8},{28,12},{1,17},{... | collective-permute-start | bytes 307208 | tf_op jit(solution)/shard_map/ppermute | solution.py:361
  13.8 0.0 collective-permute-done.10
  13.8 8.3 %collective-permute-start.1 = (bf16[48,2176]{1,0:T(8,128)(2,1)S(1)}, bf16[48,2176]{1,0:T(8,128)(2,1)S(1)}, u32[]{:S(2)}, u32[]{:S(2)}) collective-permute-start(bf16[48,2176]{1,0:T(8,128)(2,1)S(1)} %get-tuple-element.43), channel_id=1, source_target_pairs={{0,8},{4,12},{8,0},{12,4},{16,24},{20,28},{24,16},{28,20},{1,9},{5... | collective-permute-start | bytes 626696 | tf_op jit(solution)/shard_map/ppermute | solution.py:361
  22.1 0.0 collective-permute-done.9
  22.2 2.7 %collective-permute-start.2 = (bf16[48,2176]{1,0:T(8,128)(2,1)S(1)}, bf16[48,2176]{1,0:T(8,128)(2,1)S(1)}, u32[]{:S(2)}, u32[]{:S(2)}) collective-permute-start(bf16[48,2176]{1,0:T(8,128)(2,1)S(1)} %get-tuple-element.44), channel_id=1, source_target_pairs={{0,12},{4,8},{8,4},{12,0},{16,28},{20,24},{24,20},{28,16},{1,13},{... | collective-permute-start | bytes 626696 | tf_op jit(solution)/shard_map/ppermute | solution.py:361
  24.9 1.7 %collective-permute-done.8 = bf16[400,128]{1,0:T(8,128)(2,1)S(1)} collective-permute-done((bf16[400,128]{1,0:T(8,128)(2,1)S(1)}, bf16[400,128]{1,0:T(8,128)(2,1)S(1)}, u32[]{:S(2)}, u32[]{:S(2)}) %collective-permute-start.8) | collective-permute-done | bytes 102432 | tf_op jit(solution)/shard_map/ppermute | solution.py:361
  26.6 0.4 collective-permute-done.7
  27.0 0.0 collective-permute-done
  27.0 4.1 %collective-permute-done.1 = bf16[48,2176]{1,0:T(8,128)(2,1)S(1)} collective-permute-done((bf16[48,2176]{1,0:T(8,128)(2,1)S(1)}, bf16[48,2176]{1,0:T(8,128)(2,1)S(1)}, u32[]{:S(2)}, u32[]{:S(2)}) %collective-permute-start.1) | collective-permute-done | bytes 208928 | tf_op jit(solution)/shard_map/ppermute | solution.py:361
  31.2 3.2 %collective-permute-done.2 = bf16[48,2176]{1,0:T(8,128)(2,1)S(1)} collective-permute-done((bf16[48,2176]{1,0:T(8,128)(2,1)S(1)}, bf16[48,2176]{1,0:T(8,128)(2,1)S(1)}, u32[]{:S(2)}, u32[]{:S(2)}) %collective-permute-start.2) | collective-permute-done | bytes 208928 | tf_op jit(solution)/shard_map/ppermute | solution.py:361
  34.4 0.1 collective-permute-start.3
  34.5 1.6 %collective-permute-start.11 = (bf16[1536,128]{1,0:T(8,128)(2,1)S(1)}, bf16[1536,128]{1,0:T(8,128)(2,1)S(1)}, u32[]{:S(2)}, u32[]{:S(2)}) collective-permute-start(bf16[1536,128]{1,0:T(8,128)(2,1)S(1)} %pad_maximum_fusion.refs_0_), channel_id=1, source_target_pairs={{0,2},{1,3},{2,0},{3,1},{4,6},{5,7},{6,4},{7,5},{8,10},{9,11},{10,... | collective-permute-start | bytes 1179656 | tf_op jit(solution)/shard_map/ppermute | solution.py:372
  36.1 0.2 collective-permute-start.12
  36.3 9.8 %collective-permute-done.11.refs_1_ = bf16[1536,128]{1,0:T(8,128)(2,1)S(1)} collective-permute-done((bf16[1536,128]{1,0:T(8,128)(2,1)S(1)}, bf16[1536,128]{1,0:T(8,128)(2,1)S(1)}, u32[]{:S(2)}, u32[]{:S(2)}) %collective-permute-start.11) | collective-permute-done | bytes 393248 | tf_op jit(solution)/shard_map/ppermute | solution.py:372
  46.1 0.0 collective-permute-start.13
  46.1 0.0 copy-start
  46.1 0.0 copy-start.1
  46.1 0.0 copy-start.2
  46.1 1.8 %shard_map.111.refs_5_.refs_7_ = bf16[512,2048]{1,0:T(8,128)(2,1)S(1)} custom-call(bf16[512,2048]{1,0:T(8,128)(2,1)} %bitcast.17), custom_call_target="tpu_custom_call" | custom-call | flops 1000000000 | bytes 4194304 | tf_op jit(solution)/shard_map/pallas_call | solution.py:31
  47.9 0.0 collective-permute-done.3.refs_2_
  47.9 0.4 copy-done
  48.3 0.6 copy-done.1
  48.9 0.0 copy-done.2
  48.9 4.4 %shard_map.112 = (bf16[384,2048]{1,0:T(8,128)(2,1)}, bf16[384,2048]{1,0:T(8,128)(2,1)}, bf16[384,512]{1,0:T(8,128)(2,1)S(1)}, bf16[384,512]{1,0:T(8,128)(2,1)S(1...) custom-call(bf16[48,4224]{1,0:T(8,128)(2,1)S(1)} %get-tuple-element., ...), custom_call_target="tpu_custom_call" | custom-call | flops 2013265920 | bytes 13127680 | tf_op jit(solution)/shard_map/pallas_call | solution.py:31
  53.3 0.0 collective-permute-done.12.refs_2_
  53.3 0.0 collective-permute-done.13.refs_3_
  53.3 4.5 %shard_map.115 = (bf16[384,2048]{1,0:T(8,128)(2,1)}, bf16[384,2048]{1,0:T(8,128)(2,1)}, bf16[384,512]{1,0:T(8,128)(2,1)S(1)}, bf16[384,512]{1,0:T(8,128)(2,1)S(1...) custom-call(bf16[1536,128]{1,0:T(8,128)(2,1)S(1)} %pad_maximum_fusio, ...), custom_call_target="tpu_custom_call", output_to_operand_aliasing={{0}: (13, {}), {1}: (14, {}), {2}: (15, {}), {3}: (16, {}),... | custom-call | flops 2013265920 | bytes 17448960 | tf_op jit(solution)/shard_map/pallas_call | solution.py:31
  57.8 0.6 collective-permute-start.15
  58.4 0.1 collective-permute-start.5
  58.5 0.4 collective-permute-start.14
  58.9 0.6 collective-permute-done.15.b
  59.5 1.6 %collective-permute-start.16 = (bf16[200,512]{1,0:T(8,128)(2,1)S(1)}, bf16[200,512]{1,0:T(8,128)(2,1)S(1)}, u32[]{:S(2)}, u32[]{:S(2)}) collective-permute-start(bf16[200,512]{1,0:T(8,128)(2,1)S(1)} %shard_map.117), channel_id=1, source_target_pairs={{0,2},{1,3},{2,0},{3,1},{4,6},{5,7},{6,4},{7,5},{8,10},{9,11},{10,... | collective-permute-start | bytes 614408 | tf_op jit(solution)/shard_map/ppermute | solution.py:399
  61.1 0.1 collective-permute-start.4
  61.2 0.0 collective-permute-done.5.b
  61.3 0.6 collective-permute-start.6
  61.8 0.7 collective-permute-done.4.b
  62.6 0.0 collective-permute-done.14.b
  62.6 0.1 shard_map.116.refs_2_
  62.7 8.5 %collective-permute-done.6.refs_1_ = bf16[192,512]{1,0:T(8,128)(2,1)S(1)} collective-permute-done((bf16[192,512]{1,0:T(8,128)(2,1)S(1)}, bf16[192,512]{1,0:T(8,128)(2,1)S(1)}, u32[]{:S(2)}, u32[]{:S(2)}) %collective-permute-start.6) | collective-permute-done | bytes 196640 | tf_op jit(solution)/shard_map/ppermute | solution.py:399
  71.2 0.0 collective-permute-done.16.refs_3_
  71.2 0.9 shard_map.118
  72.1 3.5 %all-to-all-start = ((bf16[8,56,512]{2,1,0:T(8,128)(2,1)}), bf16[8,56,512]{2,1,0:T(8,128)(2,1)S(1)}, u32[]{:S(2)}, u32[]{:S(2)}) async-start(bf16[8,56,512]{2,1,0:T(8,128)(2,1)} %shard_map.118), calls=%async_computation | async-start | bytes 917504 | tf_op jit(solution)/shard_map/all_to_all | solution.py:406
  75.5 4.9 %shard_map.121 = f32[512,2048]{1,0:T(8,128)} custom-call(bf16[384,2048]{1,0:T(8,128)(2,1)} %get-tuple-element.73.cots, bf16[384,512]{1,0:T(8,128)(2,1)S(1)} %get-tuple-element.74.act), custom_call_target="tpu_custom_call" | custom-call | flops 805306368 | bytes 4194304 | tf_op jit(solution)/shard_map/pallas_call | solution.py:290
  80.4 5.8 %shard_map.120 = (f32[2048,512]{1,0:T(8,128)}, f32[2048,512]{1,0:T(8,128)}) custom-call(bf16[384,2048]{1,0:T(8,128)(2,1)} %get-tuple-element.68.rows, bf16[384,512]{1,0:T(8,128)(2,1)S(1)} %get-tuple-element.69.d_gate, bf16[384,512]{1,0:T(8,128)(2,1)S(1)} %get-tuple-element.70.d_up), custom_call_target="tpu_custom_call" | custom-call | flops 1610612736 | bytes 8388608 | tf_op jit(solution)/shard_map/pallas_call | solution.py:290
  86.2 2.3 %all-to-all-done.back = bf16[8,56,512]{2,1,0:T(8,128)(2,1)S(1)} async-done(((bf16[8,56,512]{2,1,0:T(8,128)(2,1)}), bf16[8,56,512]{2,1,0:T(8,128)(2,1)S(1)}, u32[]{:S(2)}, u32[]{:S(2)}) %all-to-all-start) | async-done | bytes 458784 | tf_op jit(solution)/shard_map/all_to_all | solution.py:406
  88.5 1.1 %shard_map.119 = (bf16[128,512]{1,0:T(8,128)(2,1)}, f32[8,512]{1,0:T(8,128)}) custom-call(bf16[8,48,128]{2,1,0:T(8,128)(2,1)S(1)} %get-tuple-element.40.dispatch, bf16[8,56,512]{2,1,0:T(8,128)(2,1)S(1)} %all-to-all-done.back), custom_call_target="tpu_custom_call" | custom-call | flops 50331648 | bytes 696320 | tf_op jit(solution)/shard_map/pallas_call | solution.py:31
  (16 shorter events, 0.3 us)
Async XLA Ops:
  3.2 23.8 %collective-permute-start = (bf16[48,2176]{1,0:T(8,128)(2,1)S(1)}, bf16[48,2176]{1,0:T(8,128)(2,1)S(1)}, u32[]{:S(2)}, u32[]{:S(2)}) collective-permute-start(bf16[48,2176]{1,0:T(8,128)(2,1)S(1)} %get-tuple-element.42), channel_id=1, source_target_pairs={{0,4},{4,0},{8,12},{12,8},{16,20},{20,16},{24,28},{28,24},{1,5},{5... | collective-permute-start | bytes 626696 | tf_op jit(solution)/shard_map/ppermute | solution.py:361
  6.2 7.7 %collective-permute-start.10 = (bf16[400,128]{1,0:T(8,128)(2,1)S(1)}, bf16[400,128]{1,0:T(8,128)(2,1)S(1)}, u32[]{:S(2)}, u32[]{:S(2)}) collective-permute-start(bf16[400,128]{1,0:T(8,128)(2,1)S(1)} %get-tuple-element.52), channel_id=1, source_target_pairs={{0,28},{4,24},{8,20},{12,16},{16,12},{20,8},{24,4},{28,0},{1,29},{... | collective-permute-start | bytes 307208 | tf_op jit(solution)/shard_map/ppermute | solution.py:361
  9.8 12.4 %collective-permute-start.9 = (bf16[400,128]{1,0:T(8,128)(2,1)S(1)}, bf16[400,128]{1,0:T(8,128)(2,1)S(1)}, u32[]{:S(2)}, u32[]{:S(2)}) collective-permute-start(bf16[400,128]{1,0:T(8,128)(2,1)S(1)} %get-tuple-element.51), channel_id=1, source_target_pairs={{0,24},{4,28},{8,16},{12,20},{16,8},{20,12},{24,0},{28,4},{1,25},{... | collective-permute-start | bytes 307208 | tf_op jit(solution)/shard_map/ppermute | solution.py:361
  9.8 16.8 %collective-permute-start.8 = (bf16[400,128]{1,0:T(8,128)(2,1)S(1)}, bf16[400,128]{1,0:T(8,128)(2,1)S(1)}, u32[]{:S(2)}, u32[]{:S(2)}) collective-permute-start(bf16[400,128]{1,0:T(8,128)(2,1)S(1)} %get-tuple-element.50), channel_id=1, source_target_pairs={{0,20},{4,16},{8,28},{12,24},{16,4},{20,0},{24,12},{28,8},{1,21},{... | collective-permute-start | bytes 307208 | tf_op jit(solution)/shard_map/ppermute | solution.py:361
  11.7 15.3 %collective-permute-start.7 = (bf16[400,128]{1,0:T(8,128)(2,1)S(1)}, bf16[400,128]{1,0:T(8,128)(2,1)S(1)}, u32[]{:S(2)}, u32[]{:S(2)}) collective-permute-start(bf16[400,128]{1,0:T(8,128)(2,1)S(1)} %get-tuple-element.49), channel_id=1, source_target_pairs={{0,16},{4,20},{8,24},{12,28},{16,0},{20,4},{24,8},{28,12},{1,17},{... | collective-permute-start | bytes 307208 | tf_op jit(solution)/shard_map/ppermute | solution.py:361
  13.8 17.3 %collective-permute-start.1 = (bf16[48,2176]{1,0:T(8,128)(2,1)S(1)}, bf16[48,2176]{1,0:T(8,128)(2,1)S(1)}, u32[]{:S(2)}, u32[]{:S(2)}) collective-permute-start(bf16[48,2176]{1,0:T(8,128)(2,1)S(1)} %get-tuple-element.43), channel_id=1, source_target_pairs={{0,8},{4,12},{8,0},{12,4},{16,24},{20,28},{24,16},{28,20},{1,9},{5... | collective-permute-start | bytes 626696 | tf_op jit(solution)/shard_map/ppermute | solution.py:361
  22.2 12.2 %collective-permute-start.2 = (bf16[48,2176]{1,0:T(8,128)(2,1)S(1)}, bf16[48,2176]{1,0:T(8,128)(2,1)S(1)}, u32[]{:S(2)}, u32[]{:S(2)}) collective-permute-start(bf16[48,2176]{1,0:T(8,128)(2,1)S(1)} %get-tuple-element.44), channel_id=1, source_target_pairs={{0,12},{4,8},{8,4},{12,0},{16,28},{20,24},{24,20},{28,16},{1,13},{... | collective-permute-start | bytes 626696 | tf_op jit(solution)/shard_map/ppermute | solution.py:361
  34.4 13.5 %collective-permute-start.3 = (bf16[144,2176]{1,0:T(8,128)(2,1)S(1)}, bf16[144,2176]{1,0:T(8,128)(2,1)S(1)}, u32[]{:S(2)}, u32[]{:S(2)}) collective-permute-start(bf16[144,2176]{1,0:T(8,128)(2,1)S(1)} %constant_dynamic-update-slice_fusion.refs_1_), channel_id=1, source_target_pairs={{0,1},{1,0},{2,3},{3,2},{4,5},{5,4},{6,7},{7,6},{8,9},{9,8},{10,11... | collective-permute-start | bytes 1880072 | tf_op jit(solution)/shard_map/ppermute | solution.py:368
  34.5 11.6 %collective-permute-start.11 = (bf16[1536,128]{1,0:T(8,128)(2,1)S(1)}, bf16[1536,128]{1,0:T(8,128)(2,1)S(1)}, u32[]{:S(2)}, u32[]{:S(2)}) collective-permute-start(bf16[1536,128]{1,0:T(8,128)(2,1)S(1)} %pad_maximum_fusion.refs_0_), channel_id=1, source_target_pairs={{0,2},{1,3},{2,0},{3,1},{4,6},{5,7},{6,4},{7,5},{8,10},{9,11},{10,... | collective-permute-start | bytes 1179656 | tf_op jit(solution)/shard_map/ppermute | solution.py:372
  36.1 17.2 %collective-permute-start.12 = (bf16[1536,128]{1,0:T(8,128)(2,1)S(1)}, bf16[1536,128]{1,0:T(8,128)(2,1)S(1)}, u32[]{:S(2)}, u32[]{:S(2)}) collective-permute-start(bf16[1536,128]{1,0:T(8,128)(2,1)S(1)} %pad_maximum_fusion.refs_0_), channel_id=1, source_target_pairs={{0,1},{1,0},{2,3},{3,2},{4,5},{5,4},{6,7},{7,6},{8,9},{9,8},{10,11... | collective-permute-start | bytes 1179656 | tf_op jit(solution)/shard_map/ppermute | solution.py:373
  46.1 7.2 %collective-permute-start.13 = (bf16[1536,128]{1,0:T(8,128)(2,1)S(1)}, bf16[1536,128]{1,0:T(8,128)(2,1)S(1)}, u32[]{:S(2)}, u32[]{:S(2)}) collective-permute-start(bf16[1536,128]{1,0:T(8,128)(2,1)S(1)} %collective-permute-done.11.refs_1_), channel_id=1, source_target_pairs={{0,1},{1,0},{2,3},{3,2},{4,5},{5,4},{6,7},{7,6},{8,9},{9,8},{10,11... | collective-permute-start | bytes 1179656 | tf_op jit(solution)/shard_map/ppermute | solution.py:374
  46.1 2.2 %copy-start = (bf16[1,2048,512]{2,1,0:T(8,128)(2,1)S(1)}, bf16[1,2048,512]{2,1,0:T(8,128)(2,1)}, u32[]{:S(2)}) copy-start(bf16[1,2048,512]{2,1,0:T(8,128)(2,1)} %param.10) | copy-start | bytes 6291460
  46.1 2.9 %copy-start.1 = (bf16[1,2048,512]{2,1,0:T(8,128)(2,1)S(1)}, bf16[1,2048,512]{2,1,0:T(8,128)(2,1)}, u32[]{:S(2)}) copy-start(bf16[1,2048,512]{2,1,0:T(8,128)(2,1)} %param.11) | copy-start | bytes 6291460
  46.1 2.9 %copy-start.2 = (bf16[2048,8]{0,1:T(8,128)(2,1)S(1)}, bf16[2048,8]{0,1:T(8,128)(2,1)}, u32[]{:S(2)}) copy-start(bf16[2048,8]{0,1:T(8,128)(2,1)} %param.9) | copy-start | bytes 98308
  57.8 1.6 %collective-permute-start.15 = (bf16[200,512]{1,0:T(8,128)(2,1)S(1)}, bf16[200,512]{1,0:T(8,128)(2,1)S(1)}, u32[]{:S(2)}, u32[]{:S(2)}) collective-permute-start(bf16[200,512]{1,0:T(8,128)(2,1)S(1)} %get-tuple-element.65), channel_id=1, source_target_pairs={{0,1},{1,0},{2,3},{3,2},{4,5},{5,4},{6,7},{7,6},{8,9},{9,8},{10,11... | collective-permute-start | bytes 614408 | tf_op jit(solution)/shard_map/ppermute | solution.py:397
  58.4 2.8 %collective-permute-start.5 = (bf16[192,512]{1,0:T(8,128)(2,1)S(1)}, bf16[192,512]{1,0:T(8,128)(2,1)S(1)}, u32[]{:S(2)}, u32[]{:S(2)}) collective-permute-start(bf16[192,512]{1,0:T(8,128)(2,1)S(1)} %get-tuple-element.48), channel_id=1, source_target_pairs={{0,1},{1,0},{2,3},{3,2},{4,5},{5,4},{6,7},{7,6},{8,9},{9,8},{10,11... | collective-permute-start | bytes 589832 | tf_op jit(solution)/shard_map/ppermute | solution.py:397
  58.5 4.2 %collective-permute-start.14 = (bf16[200,512]{1,0:T(8,128)(2,1)S(1)}, bf16[200,512]{1,0:T(8,128)(2,1)S(1)}, u32[]{:S(2)}, u32[]{:S(2)}) collective-permute-start(bf16[200,512]{1,0:T(8,128)(2,1)S(1)} %get-tuple-element.63), channel_id=1, source_target_pairs={{0,1},{1,0},{2,3},{3,2},{4,5},{5,4},{6,7},{7,6},{8,9},{9,8},{10,11... | collective-permute-start | bytes 614408 | tf_op jit(solution)/shard_map/ppermute | solution.py:397
  59.5 11.6 %collective-permute-start.16 = (bf16[200,512]{1,0:T(8,128)(2,1)S(1)}, bf16[200,512]{1,0:T(8,128)(2,1)S(1)}, u32[]{:S(2)}, u32[]{:S(2)}) collective-permute-start(bf16[200,512]{1,0:T(8,128)(2,1)S(1)} %shard_map.117), channel_id=1, source_target_pairs={{0,2},{1,3},{2,0},{3,1},{4,6},{5,7},{6,4},{7,5},{8,10},{9,11},{10,... | collective-permute-start | bytes 614408 | tf_op jit(solution)/shard_map/ppermute | solution.py:399
  61.1 1.4 %collective-permute-start.4 = (bf16[192,512]{1,0:T(8,128)(2,1)S(1)}, bf16[192,512]{1,0:T(8,128)(2,1)S(1)}, u32[]{:S(2)}, u32[]{:S(2)}) collective-permute-start(bf16[192,512]{1,0:T(8,128)(2,1)S(1)} %get-tuple-element.46), channel_id=1, source_target_pairs={{0,1},{1,0},{2,3},{3,2},{4,5},{5,4},{6,7},{7,6},{8,9},{9,8},{10,11... | collective-permute-start | bytes 589832 | tf_op jit(solution)/shard_map/ppermute | solution.py:397
  61.3 9.9 %collective-permute-start.6 = (bf16[192,512]{1,0:T(8,128)(2,1)S(1)}, bf16[192,512]{1,0:T(8,128)(2,1)S(1)}, u32[]{:S(2)}, u32[]{:S(2)}) collective-permute-start(bf16[192,512]{1,0:T(8,128)(2,1)S(1)} %shard_map.114), channel_id=1, source_target_pairs={{0,2},{1,3},{2,0},{3,1},{4,6},{5,7},{6,4},{7,5},{8,10},{9,11},{10,... | collective-permute-start | bytes 589832 | tf_op jit(solution)/shard_map/ppermute | solution.py:399
  72.1 16.4 %all-to-all-start = ((bf16[8,56,512]{2,1,0:T(8,128)(2,1)}), bf16[8,56,512]{2,1,0:T(8,128)(2,1)S(1)}, u32[]{:S(2)}, u32[]{:S(2)}) async-start(bf16[8,56,512]{2,1,0:T(8,128)(2,1)} %shard_map.118), calls=%async_computation | async-start | bytes 917504 | tf_op jit(solution)/shard_map/all_to_all | solution.py:406

commit v2 on v1

--- a/solution.py
+++ b/solution.py
@@ -69,8 +69,9 @@
 
 
 def pack_kernel(order, near, experts, part, *refs):
-    sources, dispatch, blocks = refs[:4], refs[4], refs[5:-7]
-    targets, (place_at, weight_at, sems) = refs[-7:-3], refs[-3:]
+    sources, dispatch, own_weight, blocks = refs[:4], refs[4], refs[5], refs[8:-5]
+    targets = (refs[6], *refs[-5:-3], refs[7])
+    place_at, weight_at, sems = refs[-3:]
     copies = [pltpu.make_async_copy(s, t, sems.at[i]) for i, (s, t) in enumerate(zip(sources, targets))]
     for copy in copies:
         copy.start()
@@ -109,8 +110,10 @@
         pick, slot_weight = all_pick[:capacity], slot_weight[:capacity]
         dispatch[expert] = pick
         if index == 0:
-            span, start = width, 0
-        elif index < near:
+            own_weight[...] = jnp.broadcast_to(slot_weight, own_weight.shape)
+            block[...] = dot(pick, meta, (1, 0)).astype(bf16)
+            continue
+        if index < near:
             span = width // cores
             start = pl.multiple_of(lax.rem(tp_index, cores) * span, lanes)
         else:
@@ -131,9 +134,15 @@
         block[2 * tall * capacity :, :] = dot(both_t, all_pick, (1, 1)).astype(bf16)
 
 
-def stage_kernel(source, target, sem):
+def stage_kernel(source, dispatch, own_weight, tokens, cotangent, target, picks, own, sem):
     copy = pltpu.make_async_copy(source, target, sem)
     copy.start()
+    parts = [dispatch[e].astype(f32) for e in range(dispatch.shape[0])]
+    picks[...] = jnp.concatenate(parts, axis=0).T.astype(bf16)
+    width = tokens.shape[1]
+    pick = dispatch[lax.axis_index("ep")]
+    own[:, :width] = dot(pick, tokens[...], (1, 0)).astype(bf16)
+    own[:, width:] = (own_weight[:, :1] * dot(pick, cotangent[...], (1, 0))).astype(bf16)
     copy.wait()
 
 
@@ -165,7 +174,7 @@
         del refs[:count]
         return taken
 
-    sent = take(3 if group == 0 else 2 * ys + 1)
+    sent = take(4 if group == 0 else 2 * ys + 1)
     w_gate, w_up, w_down, router = take(4)
     if group:
         before = take(2 * ys)
@@ -180,12 +189,12 @@
     mine = pl.ds(group * count, count)
     act, d_gate, d_up = [r.at[mine] for r in (all_act, all_d_gate, all_d_up)]
     if group == 0:
-        own, near, swapped = sent
+        own, own_meta, near, swapped = sent
         half = width // cores
         put(rows, cots, own, 0, 0, width)
         put(rows, cots, near, own.shape[0], core * half, half)
         put(rows, cots, swapped, own.shape[0], (1 - core) * half, half)
-        packed = jnp.concatenate([own[:, 2 * width :], near[:, 2 * half :]], axis=0).astype(f32)
+        packed = jnp.concatenate([own_meta[...], near[:, 2 * half :]], axis=0).astype(f32)
         weights = packed + pltpu.roll(packed, packed.shape[1] - experts, 1)
     else:
         packed = sent[2 * ys][...].astype(f32)
@@ -302,14 +311,14 @@
     )(pltpu.with_memory_space_constraint(spread, pltpu.HBM), *held)
 
 
-def combine_kernel(dispatch, back, grad_tokens, grad_router):
-    ep_count, capacity = dispatch.shape[:2]
-    total = dot(dispatch[0], back[0, :capacity], (0, 0))
+def combine_kernel(picks, back, grad_tokens, grad_router):
+    ep_count = back.shape[0]
+    capacity = picks.shape[1] // ep_count
+    rows = jnp.concatenate([back[e, :capacity] for e in range(ep_count)], axis=0)
+    grad_tokens[...] = dot(picks[...], rows, (1, 0)).astype(bf16)
     term = back[0, capacity:].astype(f32)
     for e in range(1, ep_count):
-        total = total + dot(dispatch[e], back[e, :capacity], (0, 0))
         term = term + back[e, capacity:].astype(f32)
-    grad_tokens[...] = total.astype(bf16)
     grad_router[...] = term
 
 
@@ -337,25 +346,32 @@
         turn, flip = step
         return [(i, (i // block + turn) % (ep_count // block) * block + (i % block ^ flip)) for i in range(ep_count)]
 
-    shapes = [(capacity, 2 * width + wide)] + [(capacity, 2 * half + wide)] * (held - 1)
+    shapes = [(capacity, wide)] + [(capacity, 2 * half + wide)] * (held - 1)
     shapes += [(2 * part // lanes * capacity + 2 * experts, lanes)] * (ep_count - held)
-    dispatch, *blocks = call(
+    dispatch, own_weight, held_tokens, held_cotangent, *blocks = call(
         functools.partial(pack_kernel, order, held, experts, part),
-        [shaped((ep_count, capacity, tok_rows), bf16)] + [shaped(s, bf16) for s in shapes],
+        [shaped((ep_count, capacity, tok_rows), bf16), shaped((capacity, lanes), f32)]
+        + [shaped(tokens.shape, bf16), shaped(cotangent.shape, bf16)]
+        + [shaped(s, bf16) for s in shapes],
         (tokens, routes.T, router.T, cotangent),
         2 * tok_rows * sum(math.prod(s) for s in shapes),
         [
-            pltpu.VMEM(tokens.shape, bf16),
             pltpu.VMEM(routes.shape[::-1], i32),
             pltpu.VMEM(router.shape[::-1], bf16),
-            pltpu.VMEM(cotangent.shape, bf16),
             pltpu.VMEM((wide, tok_rows), f32),
             pltpu.VMEM((wide, tok_rows), f32),
             pltpu.SemaphoreType.DMA((4,)),
         ],
         range(4),
     )
-    (w_down,) = call(stage_kernel, [shaped(w_down.shape, bf16)], (w_down,), 10**9, [pltpu.SemaphoreType.DMA], (0,))
+    w_down, picks, own_block = call(
+        stage_kernel,
+        [shaped(w_down.shape, bf16), shaped((tok_rows, ep_count * capacity), bf16), shaped((capacity, 2 * width), bf16)],
+        (w_down, dispatch, own_weight, held_tokens, held_cotangent),
+        10**9,
+        [pltpu.SemaphoreType.DMA],
+        (0,),
+    )
     got = [blocks[0]]
     for at in range(1, ep_count):
         got.append(lax.ppermute(blocks[at], "ep", to_ep(order[at])))
@@ -365,7 +381,7 @@
         here = got[group * held : (group + 1) * held]
         if group == 0:
             near = jnp.concatenate(here[1:], axis=0)
-            sent = (here[0], near, lax.ppermute(near, "tp", to_core))
+            sent = (own_block, here[0], near, lax.ppermute(near, "tp", to_core))
         else:
             mine = jnp.concatenate([g[: -2 * experts] for g in here], axis=0)
             meta = jnp.concatenate([g[-2 * experts :] for g in here], axis=0)
@@ -417,7 +433,7 @@
     grad_tokens, grad_router = call(
         combine_kernel,
         [shaped((tok_rows, part), bf16), shaped((experts, part), f32)],
-        (dispatch, returned),
+        (picks, returned),
         2 * tok_rows * part * capacity * ep_count,
     )
     return (grad_tokens, grad_router.T, grad_gate[None], grad_up[None], grad_down[None])

time: 90 us -> 88.6 us (0.984)
  local copies, waits for them, and re-layouts: 1.12 us -> 0.12 us
    unnamed x8, local copies, waits for them, and re-layouts: 1.06 us -> 0.06 us
where the time goes in v2:
time: 88.6 us; the launch traced here: 88.2 us
  waiting for transfers between devices  31.2 us (35%)
  starting transfers between devices  30.4 us (34%)
  Pallas kernels  25.6 us (29%)
    ppermute x7, starting transfers between devices, on_device(): got.append(lax.ppermute(blocks[at], 'ep', to_ep(order[at])))  21.7 us
    pallas_call x10, Pallas kernels, call(): pl.pallas_call(kernel, out_shape=outs, in_specs=[hbm if i in in_hbm else...  14.9 us
    pallas_call x2, Pallas kernels, weight_grads(): pl.pallas_call(kernel, grid=(width // tile,), out_shape=out_shape, in_spe...  10.7 us
    ppermute x1, waiting for transfers between devices, on_device(): own = [mine] + [lax.ppermute(mine, 'tp', to_y(s)) for s in range(1, ys)]  9.78 us
    ppermute x7, waiting for transfers between devices, on_device(): got.append(lax.ppermute(blocks[at], 'ep', to_ep(order[at])))  9.39 us
    ppermute x2, waiting for transfers between devices, on_device(): lax.ppermute(pairs[s], 'tp', to_y(s))  8.48 us
    all_to_all x1, starting transfers between devices, on_device(): returned = lax.all_to_all(back, 'ep', 0, 0, tiled=True)  3.47 us
    all_to_all x1, waiting for transfers between devices, on_device(): returned = lax.all_to_all(back, 'ep', 0, 0, tiled=True)  2.27 us
  transfers between devices with their start and end apart: 18, of which 9 were waited for; matrix products, arithmetic and copies ran while one was open for 0% of the time, Pallas kernels for 19%

profile of v2, /device:TPU:0, one launch (start us, length us, event | category | flops | bytes accessed | tf_op | source)
XLA Modules:
  0.0 88.2 jit_solution(3373073938462633130)
XLA Ops:
  0.6 2.4 %shard_map.110 = (bf16[8,48,128]{2,1,0:T(8,128)(2,1)S(1)}, f32[48,128]{1,0:T(8,128)S(1)}, bf16[128,2048]{1,0:T(8,128)(2,1)S(1)}, bf16[128,2048]{1,0:T(8,128)(2,1...) custom-call(bf16[128,2048]{1,0:T(8,128)(2,1)} %refs_0_.1, ...), custom_call_target="tpu_custom_call" | custom-call | flops 134217728 | bytes 3290112 | tf_op jit(solution)/shard_map/pallas_call | solution.py:31
  3.0 3.0 %collective-permute-start = (bf16[48,2176]{1,0:T(8,128)(2,1)S(1)}, bf16[48,2176]{1,0:T(8,128)(2,1)S(1)}, u32[]{:S(2)}, u32[]{:S(2)}) collective-permute-start(bf16[48,2176]{1,0:T(8,128)(2,1)S(1)} %get-tuple-element.53), channel_id=1, source_target_pairs={{0,4},{4,0},{8,12},{12,8},{16,20},{20,16},{24,28},{28,24},{1,5},{5... | collective-permute-start | bytes 626696 | tf_op jit(solution)/shard_map/ppermute | solution.py:377
  6.1 3.6 %collective-permute-start.10 = (bf16[400,128]{1,0:T(8,128)(2,1)S(1)}, bf16[400,128]{1,0:T(8,128)(2,1)S(1)}, u32[]{:S(2)}, u32[]{:S(2)}) collective-permute-start(bf16[400,128]{1,0:T(8,128)(2,1)S(1)} %get-tuple-element.64), channel_id=1, source_target_pairs={{0,28},{4,24},{8,20},{12,16},{16,12},{20,8},{24,4},{28,0},{1,29},{... | collective-permute-start | bytes 307208 | tf_op jit(solution)/shard_map/ppermute | solution.py:377
  9.6 0.0 collective-permute-start.9
  9.7 1.9 %collective-permute-start.8 = (bf16[400,128]{1,0:T(8,128)(2,1)S(1)}, bf16[400,128]{1,0:T(8,128)(2,1)S(1)}, u32[]{:S(2)}, u32[]{:S(2)}) collective-permute-start(bf16[400,128]{1,0:T(8,128)(2,1)S(1)} %get-tuple-element.62), channel_id=1, source_target_pairs={{0,20},{4,16},{8,28},{12,24},{16,4},{20,0},{24,12},{28,8},{1,21},{... | collective-permute-start | bytes 307208 | tf_op jit(solution)/shard_map/ppermute | solution.py:377
  11.6 2.1 %collective-permute-start.7 = (bf16[400,128]{1,0:T(8,128)(2,1)S(1)}, bf16[400,128]{1,0:T(8,128)(2,1)S(1)}, u32[]{:S(2)}, u32[]{:S(2)}) collective-permute-start(bf16[400,128]{1,0:T(8,128)(2,1)S(1)} %get-tuple-element.61), channel_id=1, source_target_pairs={{0,16},{4,20},{8,24},{12,28},{16,0},{20,4},{24,8},{28,12},{1,17},{... | collective-permute-start | bytes 307208 | tf_op jit(solution)/shard_map/ppermute | solution.py:377
  13.7 0.0 collective-permute-done.10
  13.7 8.3 %collective-permute-start.1 = (bf16[48,2176]{1,0:T(8,128)(2,1)S(1)}, bf16[48,2176]{1,0:T(8,128)(2,1)S(1)}, u32[]{:S(2)}, u32[]{:S(2)}) collective-permute-start(bf16[48,2176]{1,0:T(8,128)(2,1)S(1)} %get-tuple-element.54), channel_id=1, source_target_pairs={{0,8},{4,12},{8,0},{12,4},{16,24},{20,28},{24,16},{28,20},{1,9},{5... | collective-permute-start | bytes 626696 | tf_op jit(solution)/shard_map/ppermute | solution.py:377
  22.0 0.0 collective-permute-done.9
  22.0 2.7 %collective-permute-start.2 = (bf16[48,2176]{1,0:T(8,128)(2,1)S(1)}, bf16[48,2176]{1,0:T(8,128)(2,1)S(1)}, u32[]{:S(2)}, u32[]{:S(2)}) collective-permute-start(bf16[48,2176]{1,0:T(8,128)(2,1)S(1)} %get-tuple-element.55), channel_id=1, source_target_pairs={{0,12},{4,8},{8,4},{12,0},{16,28},{20,24},{24,20},{28,16},{1,13},{... | collective-permute-start | bytes 626696 | tf_op jit(solution)/shard_map/ppermute | solution.py:377
  24.7 1.7 %collective-permute-done.8 = bf16[400,128]{1,0:T(8,128)(2,1)S(1)} collective-permute-done((bf16[400,128]{1,0:T(8,128)(2,1)S(1)}, bf16[400,128]{1,0:T(8,128)(2,1)S(1)}, u32[]{:S(2)}, u32[]{:S(2)}) %collective-permute-start.8) | collective-permute-done | bytes 102432 | tf_op jit(solution)/shard_map/ppermute | solution.py:377
  26.5 0.4 collective-permute-done.7
  26.9 0.0 collective-permute-done
  26.9 4.1 %collective-permute-done.1 = bf16[48,2176]{1,0:T(8,128)(2,1)S(1)} collective-permute-done((bf16[48,2176]{1,0:T(8,128)(2,1)S(1)}, bf16[48,2176]{1,0:T(8,128)(2,1)S(1)}, u32[]{:S(2)}, u32[]{:S(2)}) %collective-permute-start.1) | collective-permute-done | bytes 208928 | tf_op jit(solution)/shard_map/ppermute | solution.py:377
  31.0 3.2 %collective-permute-done.2 = bf16[48,2176]{1,0:T(8,128)(2,1)S(1)} collective-permute-done((bf16[48,2176]{1,0:T(8,128)(2,1)S(1)}, bf16[48,2176]{1,0:T(8,128)(2,1)S(1)}, u32[]{:S(2)}, u32[]{:S(2)}) %collective-permute-start.2) | collective-permute-done | bytes 208928 | tf_op jit(solution)/shard_map/ppermute | solution.py:377
  34.2 0.0 copy-start
  34.2 0.0 copy-start.1
  34.2 0.0 copy-start.2
  34.3 0.1 collective-permute-start.3
  34.4 1.6 %collective-permute-start.11 = (bf16[1536,128]{1,0:T(8,128)(2,1)S(1)}, bf16[1536,128]{1,0:T(8,128)(2,1)S(1)}, u32[]{:S(2)}, u32[]{:S(2)}) collective-permute-start(bf16[1536,128]{1,0:T(8,128)(2,1)S(1)} %pad_maximum_fusion.refs_0_), channel_id=1, source_target_pairs={{0,2},{1,3},{2,0},{3,1},{4,6},{5,7},{6,4},{7,5},{8,10},{9,11},{10,... | collective-permute-start | bytes 1179656 | tf_op jit(solution)/shard_map/ppermute | solution.py:388
  36.0 0.2 collective-permute-start.12
  36.2 9.8 %collective-permute-done.11.refs_1_ = bf16[1536,128]{1,0:T(8,128)(2,1)S(1)} collective-permute-done((bf16[1536,128]{1,0:T(8,128)(2,1)S(1)}, bf16[1536,128]{1,0:T(8,128)(2,1)S(1)}, u32[]{:S(2)}, u32[]{:S(2)}) %collective-permute-start.11) | collective-permute-done | bytes 393248 | tf_op jit(solution)/shard_map/ppermute | solution.py:388
  45.9 0.0 collective-permute-start.13
  46.0 1.7 %shard_map.111 = (bf16[512,2048]{1,0:T(8,128)(2,1)S(1)}, bf16[128,384]{1,0:T(8,128)(2,1)S(1)}, bf16[48,4096]{1,0:T(8,128)(2,1)S(1)}) custom-call(bf16[512,2048]{1,0:T(8,128)(2,1)} %bitcast.18, bf16[8,48,128]{2,1,0:T(8,128)(2,1)S(1)} %get-tuple-element.46.dispatch, f32[48,128]{1,0:T(8,128)S(1)} %get-tuple-element.47.own_weight, ...), custom_call_target="tpu_custom_call" | custom-call | flops 1000000000 | bytes 5857280 | tf_op jit(solution)/shard_map/pallas_call | solution.py:31
  47.7 0.0 collective-permute-done.3.refs_3_
  47.7 0.0 copy-done
  47.7 0.0 copy-done.1
  47.7 0.0 copy-done.2
  47.7 4.4 %shard_map.112 = (bf16[384,2048]{1,0:T(8,128)(2,1)}, bf16[384,2048]{1,0:T(8,128)(2,1)}, bf16[384,512]{1,0:T(8,128)(2,1)S(1)}, bf16[384,512]{1,0:T(8,128)(2,1)S(1...) custom-call(bf16[48,4096]{1,0:T(8,128)(2,1)S(1)} %get-tuple-element., ...), custom_call_target="tpu_custom_call" | custom-call | flops 2013265920 | bytes 13127680 | tf_op jit(solution)/shard_map/pallas_call | solution.py:31
  52.1 0.0 collective-permute-done.12.refs_2_
  52.1 0.0 collective-permute-done.13.refs_3_
  52.2 4.5 %shard_map.115 = (bf16[384,2048]{1,0:T(8,128)(2,1)}, bf16[384,2048]{1,0:T(8,128)(2,1)}, bf16[384,512]{1,0:T(8,128)(2,1)S(1)}, bf16[384,512]{1,0:T(8,128)(2,1)S(1...) custom-call(bf16[1536,128]{1,0:T(8,128)(2,1)S(1)} %pad_maximum_fusio, ...), custom_call_target="tpu_custom_call", output_to_operand_aliasing={{0}: (13, {}), {1}: (14, {}), {2}: (15, {}), {3}: (16, {}),... | custom-call | flops 2013265920 | bytes 17448960 | tf_op jit(solution)/shard_map/pallas_call | solution.py:31
  56.6 0.6 collective-permute-start.15
  57.2 0.1 collective-permute-start.5
  57.3 0.4 collective-permute-start.14
  57.7 0.6 collective-permute-done.15.b
  58.4 1.6 %collective-permute-start.16 = (bf16[200,512]{1,0:T(8,128)(2,1)S(1)}, bf16[200,512]{1,0:T(8,128)(2,1)S(1)}, u32[]{:S(2)}, u32[]{:S(2)}) collective-permute-start(bf16[200,512]{1,0:T(8,128)(2,1)S(1)} %shard_map.117), channel_id=1, source_target_pairs={{0,2},{1,3},{2,0},{3,1},{4,6},{5,7},{6,4},{7,5},{8,10},{9,11},{10,... | collective-permute-start | bytes 614408 | tf_op jit(solution)/shard_map/ppermute | solution.py:415
  60.0 0.1 collective-permute-start.4
  60.0 0.0 collective-permute-done.5.b
  60.1 0.6 collective-permute-start.6
  60.7 0.7 collective-permute-done.4.b
  61.4 0.0 collective-permute-done.14.b
  61.5 0.1 shard_map.116.refs_2_
  61.5 8.5 %collective-permute-done.6.refs_1_ = bf16[192,512]{1,0:T(8,128)(2,1)S(1)} collective-permute-done((bf16[192,512]{1,0:T(8,128)(2,1)S(1)}, bf16[192,512]{1,0:T(8,128)(2,1)S(1)}, u32[]{:S(2)}, u32[]{:S(2)}) %collective-permute-start.6) | collective-permute-done | bytes 196640 | tf_op jit(solution)/shard_map/ppermute | solution.py:415
  70.0 0.0 collective-permute-done.16.refs_3_
  70.0 0.9 %shard_map.118 = bf16[8,56,512]{2,1,0:T(8,128)(2,1)} custom-call(bf16[192,512]{1,0:T(8,128)(2,1)S(1)} %shard_map.113.refs_0_, bf16[192,512]{1,0:T(8,128)(2,1)S(1)} %collective-permute-done.6.refs_1_, bf16[200,512]{1,0:T(8,128)(2,1)S(1)} %shard_map.116.refs_2_, bf16[200,512]{1,0:T(8,128)(2,1)S(1)} %collective-permute-done.16.refs_3_), custom_call_target="tpu_custom_call" | custom-call | flops 98304 | bytes 1261568 | tf_op jit(solution)/shard_map/pallas_call | solution.py:31
  70.9 3.5 %all-to-all-start = ((bf16[8,56,512]{2,1,0:T(8,128)(2,1)}), bf16[8,56,512]{2,1,0:T(8,128)(2,1)S(1)}, u32[]{:S(2)}, u32[]{:S(2)}) async-start(bf16[8,56,512]{2,1,0:T(8,128)(2,1)} %shard_map.118), calls=%async_computation | async-start | bytes 917504 | tf_op jit(solution)/shard_map/all_to_all | solution.py:422
  74.4 4.9 %shard_map.121 = f32[512,2048]{1,0:T(8,128)} custom-call(bf16[384,2048]{1,0:T(8,128)(2,1)} %get-tuple-element.85.cots, bf16[384,512]{1,0:T(8,128)(2,1)S(1)} %get-tuple-element.86.act), custom_call_target="tpu_custom_call" | custom-call | flops 805306368 | bytes 4194304 | tf_op jit(solution)/shard_map/pallas_call | solution.py:299
  79.3 5.8 %shard_map.120 = (f32[2048,512]{1,0:T(8,128)}, f32[2048,512]{1,0:T(8,128)}) custom-call(bf16[384,2048]{1,0:T(8,128)(2,1)} %get-tuple-element.80.rows, bf16[384,512]{1,0:T(8,128)(2,1)S(1)} %get-tuple-element.81.d_gate, bf16[384,512]{1,0:T(8,128)(2,1)S(1)} %get-tuple-element.82.d_up), custom_call_target="tpu_custom_call" | custom-call | flops 1610612736 | bytes 8388608 | tf_op jit(solution)/shard_map/pallas_call | solution.py:299
  85.1 2.3 %all-to-all-done.back = bf16[8,56,512]{2,1,0:T(8,128)(2,1)S(1)} async-done(((bf16[8,56,512]{2,1,0:T(8,128)(2,1)}), bf16[8,56,512]{2,1,0:T(8,128)(2,1)S(1)}, u32[]{:S(2)}, u32[]{:S(2)}) %all-to-all-start) | async-done | bytes 458784 | tf_op jit(solution)/shard_map/all_to_all | solution.py:422
  87.3 0.9 %shard_map.119 = (bf16[128,512]{1,0:T(8,128)(2,1)}, f32[8,512]{1,0:T(8,128)}) custom-call(bf16[128,384]{1,0:T(8,128)(2,1)S(1)} %get-tuple-element.50.picks, bf16[8,56,512]{2,1,0:T(8,128)(2,1)S(1)} %all-to-all-done.back), custom_call_target="tpu_custom_call" | custom-call | flops 50331648 | bytes 696320 | tf_op jit(solution)/shard_map/pallas_call | solution.py:31
  (16 shorter events, 0.3 us)
Async XLA Ops:
  3.0 23.8 %collective-permute-start = (bf16[48,2176]{1,0:T(8,128)(2,1)S(1)}, bf16[48,2176]{1,0:T(8,128)(2,1)S(1)}, u32[]{:S(2)}, u32[]{:S(2)}) collective-permute-start(bf16[48,2176]{1,0:T(8,128)(2,1)S(1)} %get-tuple-element.53), channel_id=1, source_target_pairs={{0,4},{4,0},{8,12},{12,8},{16,20},{20,16},{24,28},{28,24},{1,5},{5... | collective-permute-start | bytes 626696 | tf_op jit(solution)/shard_map/ppermute | solution.py:377
  6.1 7.7 %collective-permute-start.10 = (bf16[400,128]{1,0:T(8,128)(2,1)S(1)}, bf16[400,128]{1,0:T(8,128)(2,1)S(1)}, u32[]{:S(2)}, u32[]{:S(2)}) collective-permute-start(bf16[400,128]{1,0:T(8,128)(2,1)S(1)} %get-tuple-element.64), channel_id=1, source_target_pairs={{0,28},{4,24},{8,20},{12,16},{16,12},{20,8},{24,4},{28,0},{1,29},{... | collective-permute-start | bytes 307208 | tf_op jit(solution)/shard_map/ppermute | solution.py:377
  9.6 12.4 %collective-permute-start.9 = (bf16[400,128]{1,0:T(8,128)(2,1)S(1)}, bf16[400,128]{1,0:T(8,128)(2,1)S(1)}, u32[]{:S(2)}, u32[]{:S(2)}) collective-permute-start(bf16[400,128]{1,0:T(8,128)(2,1)S(1)} %get-tuple-element.63), channel_id=1, source_target_pairs={{0,24},{4,28},{8,16},{12,20},{16,8},{20,12},{24,0},{28,4},{1,25},{... | collective-permute-start | bytes 307208 | tf_op jit(solution)/shard_map/ppermute | solution.py:377
  9.7 16.8 %collective-permute-start.8 = (bf16[400,128]{1,0:T(8,128)(2,1)S(1)}, bf16[400,128]{1,0:T(8,128)(2,1)S(1)}, u32[]{:S(2)}, u32[]{:S(2)}) collective-permute-start(bf16[400,128]{1,0:T(8,128)(2,1)S(1)} %get-tuple-element.62), channel_id=1, source_target_pairs={{0,20},{4,16},{8,28},{12,24},{16,4},{20,0},{24,12},{28,8},{1,21},{... | collective-permute-start | bytes 307208 | tf_op jit(solution)/shard_map/ppermute | solution.py:377
  11.6 15.3 %collective-permute-start.7 = (bf16[400,128]{1,0:T(8,128)(2,1)S(1)}, bf16[400,128]{1,0:T(8,128)(2,1)S(1)}, u32[]{:S(2)}, u32[]{:S(2)}) collective-permute-start(bf16[400,128]{1,0:T(8,128)(2,1)S(1)} %get-tuple-element.61), channel_id=1, source_target_pairs={{0,16},{4,20},{8,24},{12,28},{16,0},{20,4},{24,8},{28,12},{1,17},{... | collective-permute-start | bytes 307208 | tf_op jit(solution)/shard_map/ppermute | solution.py:377
  13.7 17.3 %collective-permute-start.1 = (bf16[48,2176]{1,0:T(8,128)(2,1)S(1)}, bf16[48,2176]{1,0:T(8,128)(2,1)S(1)}, u32[]{:S(2)}, u32[]{:S(2)}) collective-permute-start(bf16[48,2176]{1,0:T(8,128)(2,1)S(1)} %get-tuple-element.54), channel_id=1, source_target_pairs={{0,8},{4,12},{8,0},{12,4},{16,24},{20,28},{24,16},{28,20},{1,9},{5... | collective-permute-start | bytes 626696 | tf_op jit(solution)/shard_map/ppermute | solution.py:377
  22.0 12.2 %collective-permute-start.2 = (bf16[48,2176]{1,0:T(8,128)(2,1)S(1)}, bf16[48,2176]{1,0:T(8,128)(2,1)S(1)}, u32[]{:S(2)}, u32[]{:S(2)}) collective-permute-start(bf16[48,2176]{1,0:T(8,128)(2,1)S(1)} %get-tuple-element.55), channel_id=1, source_target_pairs={{0,12},{4,8},{8,4},{12,0},{16,28},{20,24},{24,20},{28,16},{1,13},{... | collective-permute-start | bytes 626696 | tf_op jit(solution)/shard_map/ppermute | solution.py:377
  34.2 13.5 %copy-start = (bf16[1,2048,512]{2,1,0:T(8,128)(2,1)S(1)}, bf16[1,2048,512]{2,1,0:T(8,128)(2,1)}, u32[]{:S(2)}) copy-start(bf16[1,2048,512]{2,1,0:T(8,128)(2,1)} %param.10) | copy-start | bytes 6291460
  34.2 13.5 %copy-start.1 = (bf16[1,2048,512]{2,1,0:T(8,128)(2,1)S(1)}, bf16[1,2048,512]{2,1,0:T(8,128)(2,1)}, u32[]{:S(2)}) copy-start(bf16[1,2048,512]{2,1,0:T(8,128)(2,1)} %param.11) | copy-start | bytes 6291460
  34.2 13.5 %copy-start.2 = (bf16[2048,8]{0,1:T(8,128)(2,1)S(1)}, bf16[2048,8]{0,1:T(8,128)(2,1)}, u32[]{:S(2)}) copy-start(bf16[2048,8]{0,1:T(8,128)(2,1)} %param.9) | copy-start | bytes 98308
  34.3 13.4 %collective-permute-start.3 = (bf16[144,2176]{1,0:T(8,128)(2,1)S(1)}, bf16[144,2176]{1,0:T(8,128)(2,1)S(1)}, u32[]{:S(2)}, u32[]{:S(2)}) collective-permute-start(bf16[144,2176]{1,0:T(8,128)(2,1)S(1)} %constant_dynamic-update-slice_fusion.refs_2_), channel_id=1, source_target_pairs={{0,1},{1,0},{2,3},{3,2},{4,5},{5,4},{6,7},{7,6},{8,9},{9,8},{10,11... | collective-permute-start | bytes 1880072 | tf_op jit(solution)/shard_map/ppermute | solution.py:384
  34.4 11.6 %collective-permute-start.11 = (bf16[1536,128]{1,0:T(8,128)(2,1)S(1)}, bf16[1536,128]{1,0:T(8,128)(2,1)S(1)}, u32[]{:S(2)}, u32[]{:S(2)}) collective-permute-start(bf16[1536,128]{1,0:T(8,128)(2,1)S(1)} %pad_maximum_fusion.refs_0_), channel_id=1, source_target_pairs={{0,2},{1,3},{2,0},{3,1},{4,6},{5,7},{6,4},{7,5},{8,10},{9,11},{10,... | collective-permute-start | bytes 1179656 | tf_op jit(solution)/shard_map/ppermute | solution.py:388
  36.0 16.2 %collective-permute-start.12 = (bf16[1536,128]{1,0:T(8,128)(2,1)S(1)}, bf16[1536,128]{1,0:T(8,128)(2,1)S(1)}, u32[]{:S(2)}, u32[]{:S(2)}) collective-permute-start(bf16[1536,128]{1,0:T(8,128)(2,1)S(1)} %pad_maximum_fusion.refs_0_), channel_id=1, source_target_pairs={{0,1},{1,0},{2,3},{3,2},{4,5},{5,4},{6,7},{7,6},{8,9},{9,8},{10,11... | collective-permute-start | bytes 1179656 | tf_op jit(solution)/shard_map/ppermute | solution.py:389
  45.9 6.2 %collective-permute-start.13 = (bf16[1536,128]{1,0:T(8,128)(2,1)S(1)}, bf16[1536,128]{1,0:T(8,128)(2,1)S(1)}, u32[]{:S(2)}, u32[]{:S(2)}) collective-permute-start(bf16[1536,128]{1,0:T(8,128)(2,1)S(1)} %collective-permute-done.11.refs_1_), channel_id=1, source_target_pairs={{0,1},{1,0},{2,3},{3,2},{4,5},{5,4},{6,7},{7,6},{8,9},{9,8},{10,11... | collective-permute-start | bytes 1179656 | tf_op jit(solution)/shard_map/ppermute | solution.py:390
  56.6 1.7 %collective-permute-start.15 = (bf16[200,512]{1,0:T(8,128)(2,1)S(1)}, bf16[200,512]{1,0:T(8,128)(2,1)S(1)}, u32[]{:S(2)}, u32[]{:S(2)}) collective-permute-start(bf16[200,512]{1,0:T(8,128)(2,1)S(1)} %get-tuple-element.77), channel_id=1, source_target_pairs={{0,1},{1,0},{2,3},{3,2},{4,5},{5,4},{6,7},{7,6},{8,9},{9,8},{10,11... | collective-permute-start | bytes 614408 | tf_op jit(solution)/shard_map/ppermute | solution.py:413
  57.2 2.8 %collective-permute-start.5 = (bf16[192,512]{1,0:T(8,128)(2,1)S(1)}, bf16[192,512]{1,0:T(8,128)(2,1)S(1)}, u32[]{:S(2)}, u32[]{:S(2)}) collective-permute-start(bf16[192,512]{1,0:T(8,128)(2,1)S(1)} %get-tuple-element.60), channel_id=1, source_target_pairs={{0,1},{1,0},{2,3},{3,2},{4,5},{5,4},{6,7},{7,6},{8,9},{9,8},{10,11... | collective-permute-start | bytes 589832 | tf_op jit(solution)/shard_map/ppermute | solution.py:413
  57.3 4.1 %collective-permute-start.14 = (bf16[200,512]{1,0:T(8,128)(2,1)S(1)}, bf16[200,512]{1,0:T(8,128)(2,1)S(1)}, u32[]{:S(2)}, u32[]{:S(2)}) collective-permute-start(bf16[200,512]{1,0:T(8,128)(2,1)S(1)} %get-tuple-element.75), channel_id=1, source_target_pairs={{0,1},{1,0},{2,3},{3,2},{4,5},{5,4},{6,7},{7,6},{8,9},{9,8},{10,11... | collective-permute-start | bytes 614408 | tf_op jit(solution)/shard_map/ppermute | solution.py:413
  58.4 11.6 %collective-permute-start.16 = (bf16[200,512]{1,0:T(8,128)(2,1)S(1)}, bf16[200,512]{1,0:T(8,128)(2,1)S(1)}, u32[]{:S(2)}, u32[]{:S(2)}) collective-permute-start(bf16[200,512]{1,0:T(8,128)(2,1)S(1)} %shard_map.117), channel_id=1, source_target_pairs={{0,2},{1,3},{2,0},{3,1},{4,6},{5,7},{6,4},{7,5},{8,10},{9,11},{10,... | collective-permute-start | bytes 614408 | tf_op jit(solution)/shard_map/ppermute | solution.py:415
  60.0 1.4 %collective-permute-start.4 = (bf16[192,512]{1,0:T(8,128)(2,1)S(1)}, bf16[192,512]{1,0:T(8,128)(2,1)S(1)}, u32[]{:S(2)}, u32[]{:S(2)}) collective-permute-start(bf16[192,512]{1,0:T(8,128)(2,1)S(1)} %get-tuple-element.58), channel_id=1, source_target_pairs={{0,1},{1,0},{2,3},{3,2},{4,5},{5,4},{6,7},{7,6},{8,9},{9,8},{10,11... | collective-permute-start | bytes 589832 | tf_op jit(solution)/shard_map/ppermute | solution.py:413
  60.1 9.9 %collective-permute-start.6 = (bf16[192,512]{1,0:T(8,128)(2,1)S(1)}, bf16[192,512]{1,0:T(8,128)(2,1)S(1)}, u32[]{:S(2)}, u32[]{:S(2)}) collective-permute-start(bf16[192,512]{1,0:T(8,128)(2,1)S(1)} %shard_map.114), channel_id=1, source_target_pairs={{0,2},{1,3},{2,0},{3,1},{4,6},{5,7},{6,4},{7,5},{8,10},{9,11},{10,... | collective-permute-start | bytes 589832 | tf_op jit(solution)/shard_map/ppermute | solution.py:415
  70.9 16.4 %all-to-all-start = ((bf16[8,56,512]{2,1,0:T(8,128)(2,1)}), bf16[8,56,512]{2,1,0:T(8,128)(2,1)S(1)}, u32[]{:S(2)}, u32[]{:S(2)}) async-start(bf16[8,56,512]{2,1,0:T(8,128)(2,1)} %shard_map.118), calls=%async_computation | async-start | bytes 917504 | tf_op jit(solution)/shard_map/all_to_all | solution.py:422
